TPU v7x, 512 devices: a 4x2x32 block of a 4x8x32 slice. The times are simulated.
512 devices in a mesh: grp: 2 (over y), sp: 32 (over z), tp: 8 (over x, core).
Axes of the slice: x: 4, y: 2, z: 32, core: 2. Of those that a mesh axis runs over, the one named last changes fastest.
The devices are a block of a 4x8x32 slice.
Arguments:
- latent: bfloat16 [32768, 4096], P(('grp', 'sp', 'tp')), parts along dimension 0, may hold values from -260 to 260
- context: bfloat16 [1536, 4096], P(('grp', 'sp')), parts along dimension 0, may hold values from -6 to 6
- conditioning: bfloat16 [8192], P(('grp', 'sp')), parts along dimension 0, may hold values from -6 to 6
- norm_gain: float32 [4096], replicated, may hold values from 0.1 to 1.9
- shift_weight: bfloat16 [4096, 4096], P('sp', 'tp'), may hold values from -0.09375 to 0.09375
- scale_weight: bfloat16 [4096, 4096], P('sp', 'tp'), may hold values from -0.09375 to 0.09375
- gate_weight: bfloat16 [4096, 4096], P('sp', 'tp'), may hold values from -0.09375 to 0.09375
- query_weight: bfloat16 [4096, 1024], P(None, 'tp'), may hold values from -3 to 3
- key_weight: bfloat16 [4096, 512], P(None, 'tp'), may hold values from -3 to 3
- value_weight: bfloat16 [4096, 512], P(None, 'tp'), may hold values from -0.09375 to 0.09375
- out_weight: bfloat16 [1024, 4096], P(None, 'tp'), may hold values from -1.5 to 1.5
- sink_logit: float32 [16], P('tp'), may hold values from 3 to 7
Outputs:
- mixed: bfloat16 [32768, 4096], P(('grp', 'sp', 'tp')), parts along dimension 0
There are 2 independent parts, one for each index of `grp`. A program takes and returns all parts, laid end to end along the dimension named above; an argument that names none is the same for every part. Nothing has to cross between parts.
All inputs are finite; a program needn't handle non-finite values.
Results may differ from a plain program's by a relative error of at most 0.012.
The roundings to bfloat16 on the way count: a program that leaves them out, or rounds other values in their place, can miss the bound.
Values may be sent and summed in bfloat16 or wider, within the bound.
A program may use at most 64 MiB of HBM per device.

v0:
```python
import jax
import jax.numpy as jnp
from jax import lax
from jax.sharding import PartitionSpec as P

HEADS = 16
KV_HEADS = 8
HD = 64
GRID_W = 64
WIN = 128


epsilon = 1e-06
rope_base = 10000.0
neg_large = -1e30


def sent_to_all(value, axis):
    count = lax.axis_size(axis)
    return lax.all_to_all(
        jnp.broadcast_to(value[None], (count, *value.shape)), axis, 0, 0, tiled=True
    )


def over_copies(value, axis):
    return sent_to_all(value, axis).sum(axis=0)


def packed_total(arrays, axis):
    ends = [0]
    for a in arrays:
        ends.append(ends[-1] + a.size)
    running = over_copies(jnp.concatenate([a.ravel() for a in arrays]), axis)
    return tuple((running[b:e].reshape(a.shape) for a, b, e in zip(arrays, ends, ends[1:])))


def rows_first(arrays, axis, dims):
    turned = [jnp.moveaxis(a, dim, 0) for a, dim in zip(arrays, dims)]
    both = jnp.concatenate([t.reshape(len(t), -1) for t in turned], axis=1)
    whole, at, outs = (lax.all_gather(both, axis, axis=0, tiled=True), 0, [])
    for t, dim in zip(turned, dims):
        share = whole[:, at : at + t[0].size].reshape(-1, *t.shape[1:])
        outs.append(jnp.moveaxis(share, 0, dim))
        at += t[0].size
    return tuple(outs)


def with_halo(cells, sides, width):
    for axis, dim in sides:
        count = lax.axis_size(axis)
        ends = count - 1
        head = lax.slice_in_dim(cells, 0, width, axis=dim)
        tail = lax.slice_in_dim(cells, cells.shape[dim] - width, cells.shape[dim], axis=dim)
        cells = jnp.concatenate(
            [
                lax.ppermute(tail, axis, [(i, (i + 1) % count) for i in range(ends)]),
                cells,
                lax.ppermute(head, axis, [((i + 1) % count, i) for i in range(ends)]),
            ],
            axis=dim,
        )
    return cells


def laid_out(tiles, dim):
    shape = list(tiles.shape[1:])
    shape[dim] *= tiles.shape[0]
    return jnp.moveaxis(tiles, 0, dim).reshape(shape)


def collect(value, axis, dim):
    return laid_out(sent_to_all(value, axis), dim)


def row_norm(matrix, norm_gain):
    values = matrix.astype(jnp.float32)
    return (
        values * lax.rsqrt(jnp.mean(values * values, axis=-1, keepdims=True) + epsilon) * norm_gain
    )


def axial_turn(values, position):
    half_dim = values.shape[-1] // 2
    quarter = half_dim // 2
    inverse = rope_base ** (-jnp.arange(quarter, dtype=jnp.float32) / quarter)

    def turn(section, coordinate):
        angles = coordinate.astype(jnp.float32)[:, None] * inverse[None, :]
        cosine = jnp.cos(angles)[:, None, :]
        sine_part = jnp.sin(angles)[:, None, :]
        leading = section[..., :quarter]
        trailing = section[..., quarter:]
        return jnp.concatenate(
            [leading * cosine - trailing * sine_part, leading * sine_part + trailing * cosine],
            axis=-1,
        )

    return jnp.concatenate(
        [
            turn(values[..., :half_dim], position // GRID_W),
            turn(values[..., half_dim:], position % GRID_W),
        ],
        axis=-1,
    )


def context_pairs(context_rows, norm_gain, key_weight, value_weight):
    prepared = row_norm(context_rows, norm_gain).astype(jnp.bfloat16)
    return jnp.concatenate(
        [
            jnp.dot(prepared, key_weight, preferred_element_type=jnp.float32),
            jnp.dot(prepared, value_weight, preferred_element_type=jnp.float32),
        ],
        axis=1,
    ).astype(jnp.bfloat16)


def local(
    latent,
    context,
    conditioning,
    norm_gain,
    shift_weight,
    scale_weight,
    gate_weight,
    query_weight,
    key_weight,
    value_weight,
    out_weight,
    sink_logit,
):
    lifted = jax.nn.silu(conditioning.astype(jnp.float32)).astype(jnp.bfloat16)[None, :]
    shift_part = jnp.dot(lifted, shift_weight, preferred_element_type=jnp.float32)[0]
    scale_part = jnp.dot(lifted, scale_weight, preferred_element_type=jnp.float32)[0]
    gate_part = jnp.dot(lifted, gate_weight, preferred_element_type=jnp.float32)[0]
    summed = packed_total((shift_part, scale_part, gate_part), "sp")
    shift_vec, scale_vec, gate_vec = rows_first((summed[0], summed[1], summed[2]), "tp", (0, 0, 0))
    normed = (row_norm(latent, norm_gain) * (1.0 + scale_vec) + shift_vec).astype(jnp.bfloat16)
    segment = lax.all_gather(normed, "tp", axis=0, tiled=True)
    projected = jnp.concatenate(
        [
            jnp.dot(segment, query_weight, preferred_element_type=jnp.float32),
            jnp.dot(segment, key_weight, preferred_element_type=jnp.float32),
            jnp.dot(segment, value_weight, preferred_element_type=jnp.float32),
        ],
        axis=1,
    )
    row_count = projected.shape[0]
    query_width = query_weight.shape[1]
    key_width = key_weight.shape[1]
    query_heads = query_width // HD
    pair_heads = key_width // HD
    group_size = HEADS // KV_HEADS
    row_offset = lax.axis_index("sp") * row_count
    position = row_offset + jnp.arange(row_count, dtype=jnp.int32)
    queries = axial_turn(
        projected[:, :query_width].reshape(row_count, query_heads, HD), position
    ).astype(jnp.bfloat16)
    latent_keys = axial_turn(
        projected[:, query_width : query_width + key_width].reshape(row_count, pair_heads, HD),
        position,
    ).astype(jnp.bfloat16)
    latent_values = projected[:, query_width + key_width :].astype(jnp.bfloat16)
    key_value = jnp.concatenate([latent_keys.reshape(row_count, key_width), latent_values], axis=1)
    widened = with_halo(key_value, (("sp", 0),), WIN)
    context_all = collect(context_pairs(context, norm_gain, key_weight, value_weight), "sp", 0)
    block_count = row_count // WIN
    context_count = context_all.shape[0]
    query_blocks = queries.reshape(block_count, WIN, pair_heads, group_size, HD)
    band_blocks = widened.reshape(block_count + 2, WIN, 2 * key_width)
    band_rows = jnp.concatenate(
        [band_blocks[:block_count], band_blocks[1 : block_count + 1], band_blocks[2:]], axis=1
    )
    band_keys = band_rows[..., :key_width].reshape(block_count, 3 * WIN, pair_heads, HD)
    band_values = band_rows[..., key_width:].reshape(block_count, 3 * WIN, pair_heads, HD)
    context_keys = context_all[:, :key_width].reshape(context_count, pair_heads, HD)
    context_values = context_all[:, key_width:].reshape(context_count, pair_heads, HD)
    factor = HD ** (-0.5)
    local_scores = (
        jnp.einsum("nqhgd,nkhd->nhgqk", query_blocks, band_keys, preferred_element_type=jnp.float32)
        * factor
    )
    query_pos = position.reshape(block_count, WIN)
    key_pos = (
        row_offset
        - WIN
        + jnp.arange(block_count, dtype=jnp.int32)[:, None] * WIN
        + jnp.arange(3 * WIN, dtype=jnp.int32)[None, :]
    )
    seq_total = row_count * lax.axis_size("sp")
    allowed = (
        (jnp.abs(key_pos[:, None, :] - query_pos[:, :, None]) <= WIN)
        & (key_pos[:, None, :] >= 0)
        & (key_pos[:, None, :] < seq_total)
    )
    local_scores = jnp.where(allowed[:, None, None], local_scores, neg_large)
    context_scores = (
        jnp.einsum(
            "nqhgd,thd->nhgqt", query_blocks, context_keys, preferred_element_type=jnp.float32
        )
        * factor
    )
    sink_values = sink_logit.reshape(pair_heads, group_size)[None, :, :, None, None]
    highest = jnp.maximum(
        jnp.maximum(
            jnp.max(local_scores, axis=-1, keepdims=True),
            jnp.max(context_scores, axis=-1, keepdims=True),
        ),
        sink_values,
    )
    local_exp = jnp.exp(local_scores - highest)
    context_exp = jnp.exp(context_scores - highest)
    denominator = (
        jnp.sum(local_exp, axis=-1, keepdims=True)
        + jnp.sum(context_exp, axis=-1, keepdims=True)
        + jnp.exp(sink_values - highest)
    )
    local_weights = (local_exp / denominator).astype(jnp.bfloat16)
    context_weights = (context_exp / denominator).astype(jnp.bfloat16)
    attended = jnp.einsum(
        "nhgqk,nkhd->nqhgd", local_weights, band_values, preferred_element_type=jnp.float32
    ) + jnp.einsum(
        "nhgqt,thd->nqhgd", context_weights, context_values, preferred_element_type=jnp.float32
    )
    attended = attended.reshape(row_count, query_width).astype(jnp.bfloat16)
    columns_part = jnp.dot(
        collect(attended, "tp", 1), out_weight, preferred_element_type=jnp.float32
    ).astype(jnp.bfloat16)
    blended = lax.all_to_all(columns_part, "tp", split_axis=0, concat_axis=1, tiled=True)
    return (latent.astype(jnp.float32) + gate_vec * blended.astype(jnp.float32)).astype(
        jnp.bfloat16
    )


def solution(mesh):
    in_specs = (
        P(("grp", "sp", "tp"), None),
        P(("grp", "sp"), None),
        P(("grp", "sp")),
        P(),
        P("sp", "tp"),
        P("sp", "tp"),
        P("sp", "tp"),
        P(None, "tp"),
        P(None, "tp"),
        P(None, "tp"),
        P(None, "tp"),
        P("tp"),
    )
    out_specs = P(("grp", "sp", "tp"), None)
    return jax.shard_map(local, mesh=mesh, in_specs=in_specs, out_specs=out_specs, check_vma=False)
```

profile of v0, /device:TPU:33, one launch (start us, length us, event | category | flops | bytes accessed | tf_op | source)
XLA Modules:
  0.0 197.6 jit_solution(16965403692785830598)
XLA Ops:
  6.6 1.2 fusion.60
  7.8 1.1 fusion.58
  8.8 1.1 fusion.56
  9.9 0.8 broadcast_in_dim.14
  10.7 46.3 %all-to-all-start = ((f32[32,1,1536]{2,1,0:T(1,128)}), f32[32,1,1536]{2,1,0:T(1,128)S(1)}, u32[]{:S(2)}, u32[]{:S(2)}) async-start(f32[32,1,1536]{2,1,0:T(1,128)} %broadcast_in_dim.14), calls=%async_computation | async-start | bytes 393216 | tf_op jit(solution)/shard_map/all_to_all | solution.py:20
  57.0 0.1 all-gather.2.cloned.1.call-start
  57.1 1.2 fusion.12
  58.3 33.6 %all-to-all-done = f32[32,1,1536]{2,1,0:T(1,128)S(1)} async-done(((f32[32,1,1536]{2,1,0:T(1,128)}), f32[32,1,1536]{2,1,0:T(1,128)S(1)}, u32[]{:S(2)}, u32[]{:S(2)}) %all-to-all-start) | async-done | bytes 196640 | tf_op jit(solution)/shard_map/all_to_all | solution.py:20
  91.9 0.1 reduce_sum.45
  92.0 15.7 %all_gather.6 = f32[4096,3]{0,1:T(4,128)S(1)} all-gather(f32[512,3]{0,1:T(4,128)S(1)} %pad_maximum_fusion.3), channel_id=1, replica_groups=mesh['grp'=2,'sp'=32,'tp'=8] {'tp'}, dimensions={0}, use_global_device_ids=true | all-gather | bytes 55296 | tf_op jit(solution)/shard_map/all_gather | solution.py:40
  107.8 2.1 %fusion.16 = bf16[64,4096]{1,0:T(8,128)(2,1)} fusion(bf16[64,4096]{1,0:T(8,128)(2,1)} %param.12, f32[4096]{0:T(1024)S(1)} %bitcast.164, f32[4096]{0:T(1024)S(1)} %bitcast.165, f32[4096]{0:T(1024)} %param.15, f32[64]{0:T(128)S(1)} %add_rsqrt_fusion.1), kind=kLoop, calls=%fused_computation.29 | loop fusion | flops 1572864 | bytes 1097984 | tf_op jit(solution)/shard_map/convert_element_type | solution.py:138
  109.9 0.1 all-gather.2.cloned.1.call-update
  110.0 0.2 fusion.21
  110.2 0.3 convolution_convert_fusion.2
  110.5 0.3 convolution_convert_fusion.3
  110.8 0.1 pad_maximum_fusion.4
  110.9 0.7 broadcast_in_dim.17
  111.6 4.8 %all-to-all-start.1 = ((bf16[32,24,128]{2,1,0:T(8,128)(2,1)}), bf16[32,24,128]{2,1,0:T(8,128)(2,1)S(1)}, u32[]{:S(2)}, u32[]{:S(2)}) async-start(bf16[32,24,128]{2,1,0:T(8,128)(2,1)} %broadcast_in_dim.17), calls=%async_computation.1 | async-start | bytes 393216 | tf_op jit(solution)/shard_map/all_to_all | solution.py:20
  116.5 0.1 fusion.50
  116.5 0.1 iota_add_fusion
  116.6 0.3 multiply_cosine_fusion
  116.9 0.9 fusion.20
  117.9 21.9 %all-gather.2.cloned.1.call-done = bf16[512,4096]{1,0:T(8,128)(2,1)} async-done(((bf16[64,4096]{1,0:T(8,128)(2,1)}), bf16[512,4096]{1,0:T(8,128)(2,1)}) %all-gather.2.cloned.1.call-update) | async-done | bytes 4194320 | tf_op jit(solution)/shard_map/all_gather | solution.py:139
  139.8 3.7 %convolution_bitcast_fusion.1 = f32[512,1,64]{0,2,1:T(8,128)S(1)} fusion(bf16[512,4096]{1,0:T(8,128)(2,1)} %all-gather.2.cloned.1.call-done, bf16[4096,64]{0,1:T(8,128)(2,1)S(1)} %copy-done.3), kind=kOutput, calls=%fused_computation.20 | convolution fusion | flops 268435456 | bytes 4849664 | tf_op jit(solution)/shard_map/dot_general | solution.py:143
  143.5 0.2 constant_dynamic-update-slice_fusion.3
  143.7 0.2 constant_dynamic-update-slice_fusion.2
  143.9 0.2 constant_dynamic-update-slice_fusion.1
  144.1 0.2 constant_dynamic-update-slice_fusion
  144.3 1.4 fusion.11
  145.7 1.3 collective-permute-start.1
  147.0 4.2 %collective-permute-start = (bf16[128,128]{0,1:T(8,128)(2,1)S(1)}, bf16[128,128]{0,1:T(8,128)(2,1)S(1)}, u32[]{:S(2)}, u32[]{:S(2)}) collective-permute-start(bf16[128,128]{0,1:T(8,128)(2,1)S(1)} %get-tuple-element.14), channel_id=1, source_target_pairs={{0,8},{8,16},{16,24},{24,32},{32,40},{40,48},{48,56},{56,64},{64,7... | collective-permute-start | bytes 98312 | tf_op jit(solution)/shard_map/ppermute | solution.py:56
  151.3 1.5 fusion.70
  152.9 0.6 bitcast_reduce_fusion
  153.7 0.4 fusion.69
  154.1 0.1 maximum_maximum_fusion
  154.2 0.5 fusion.1
  154.8 0.2 fusion.5
  155.0 0.1 exponential_add_fusion
  155.1 0.8 fusion.7
  155.9 0.4 fusion.10
  156.3 0.1 copy.58
  156.4 0.1 broadcast_in_dim.18
  156.5 19.3 %all_to_all.29 = bf16[8,512,128]{1,2,0:T(8,128)(2,1)S(1)} all-to-all(bf16[8,512,128]{1,2,0:T(8,128)(2,1)S(1)} %broadcast_in_dim.18), channel_id=1, replica_groups=mesh['grp'=2,'sp'=32,'tp'=8] {'tp'}, dimensions={0} | all-to-all | bytes 2097152 | tf_op jit(solution)/shard_map/all_to_all | solution.py:20
  175.9 0.7 convolution_convert_fusion
  176.6 13.0 %all_to_all.30 = bf16[8,64,512]{2,1,0:T(8,128)(2,1)S(1)} all-to-all(bf16[8,64,512]{2,1,0:T(8,128)(2,1)S(1)} %bitcast.161), channel_id=1, replica_groups=mesh['grp'=2,'sp'=32,'tp'=8] {'tp'}, dimensions={0} | all-to-all | bytes 1048576 | tf_op jit(solution)/shard_map/all_to_all | solution.py:229
  189.6 0.1 convert_bitcast_fusion
  189.7 0.1 copy.79
  189.8 0.9 fusion.17
  (42 shorter events, 0.5 us)
Async XLA Ops:
  6.5 169.3 %copy-start = (bf16[1024,512]{1,0:T(8,128)(2,1)S(1)}, bf16[1024,512]{1,0:T(8,128)(2,1)}, u32[]{:S(2)}) copy-start(bf16[1024,512]{1,0:T(8,128)(2,1)} %param.22) | copy-start | bytes 3145732
  6.6 103.6 %copy-start.7 = (f32[4096]{0:T(1024)S(1)}, f32[4096]{0:T(1024)}, u32[]{:S(2)}) copy-start(f32[4096]{0:T(1024)} %param.15) | copy-start | bytes 49156
  6.6 103.4 %copy-start.5 = (bf16[24,4096]{1,0:T(8,128)(2,1)S(1)}, bf16[24,4096]{1,0:T(8,128)(2,1)}, u32[]{:S(2)}) copy-start(bf16[24,4096]{1,0:T(8,128)(2,1)} %param.13) | copy-start | bytes 589828
  6.6 103.6 %copy-start.4 = (bf16[4096,64]{0,1:T(8,128)(2,1)S(1)}, bf16[4096,64]{0,1:T(8,128)(2,1)}, u32[]{:S(2)}) copy-start(bf16[4096,64]{0,1:T(8,128)(2,1)} %param.21) | copy-start | bytes 1572868
  6.6 103.9 %copy-start.3 = (bf16[4096,64]{0,1:T(8,128)(2,1)S(1)}, bf16[4096,64]{0,1:T(8,128)(2,1)}, u32[]{:S(2)}) copy-start(bf16[4096,64]{0,1:T(8,128)(2,1)} %param.20) | copy-start | bytes 1572868
  10.7 81.2 %all-to-all-start = ((f32[32,1,1536]{2,1,0:T(1,128)}), f32[32,1,1536]{2,1,0:T(1,128)S(1)}, u32[]{:S(2)}, u32[]{:S(2)}) async-start(f32[32,1,1536]{2,1,0:T(1,128)} %broadcast_in_dim.14), calls=%async_computation | async-start | bytes 393216 | tf_op jit(solution)/shard_map/all_to_all | solution.py:20
  57.0 82.8 %all-gather.2.cloned.1.call-start = ((), (), s32[]{:S(2)}) async-start(), calls=%async_computation.4 | async-start | bytes 4718592 | tf_op jit(solution)/shard_map/all_gather | solution.py:139
  111.6 41.3 %all-to-all-start.1 = ((bf16[32,24,128]{2,1,0:T(8,128)(2,1)}), bf16[32,24,128]{2,1,0:T(8,128)(2,1)S(1)}, u32[]{:S(2)}, u32[]{:S(2)}) async-start(bf16[32,24,128]{2,1,0:T(8,128)(2,1)} %broadcast_in_dim.17), calls=%async_computation.1 | async-start | bytes 393216 | tf_op jit(solution)/shard_map/all_to_all | solution.py:20
  139.8 4.5 %copy-start.1 = (bf16[512,4096]{1,0:T(8,128)(2,1)S(1)}, bf16[512,4096]{1,0:T(8,128)(2,1)}, u32[]{:S(2)}) copy-start(bf16[512,4096]{1,0:T(8,128)(2,1)} %all-gather.2.cloned.1.call-done) | copy-start | bytes 12582916
  143.5 7.8 %copy-start.6 = (bf16[4096,128]{1,0:T(8,128)(2,1)S(1)}, bf16[4096,128]{1,0:T(8,128)(2,1)}, u32[]{:S(2)}) copy-start(bf16[4096,128]{1,0:T(8,128)(2,1)} %param.19) | copy-start | bytes 3145732
  145.7 7.8 %collective-permute-start.1 = (bf16[128,128]{0,1:T(8,128)(2,1)S(1)}, bf16[128,128]{0,1:T(8,128)(2,1)S(1)}, u32[]{:S(2)}, u32[]{:S(2)}) collective-permute-start(bf16[128,128]{0,1:T(8,128)(2,1)S(1)} %get-tuple-element.13), channel_id=1, source_target_pairs={{8,0},{16,8},{24,16},{32,24},{40,32},{48,40},{56,48},{64,56},{72,6... | collective-permute-start | bytes 98312 | tf_op jit(solution)/shard_map/ppermute | solution.py:58
  147.0 6.5 %collective-permute-start = (bf16[128,128]{0,1:T(8,128)(2,1)S(1)}, bf16[128,128]{0,1:T(8,128)(2,1)S(1)}, u32[]{:S(2)}, u32[]{:S(2)}) collective-permute-start(bf16[128,128]{0,1:T(8,128)(2,1)S(1)} %get-tuple-element.14), channel_id=1, source_target_pairs={{0,8},{8,16},{16,24},{24,32},{32,40},{40,48},{48,56},{56,64},{64,7... | collective-permute-start | bytes 98312 | tf_op jit(solution)/shard_map/ppermute | solution.py:56
  152.9 1.2 copy-start.8
  176.6 13.2 %copy-start.2 = (bf16[64,4096]{1,0:T(8,128)(2,1)S(1)}, bf16[64,4096]{1,0:T(8,128)(2,1)}, u32[]{:S(2)}) copy-start(bf16[64,4096]{1,0:T(8,128)(2,1)} %param.12) | copy-start | bytes 1572868
Sparse Core Ops, SparseCore 0:
  110.1 29.6 all-gather.1
where the time goes:
time: 198 us
  starting transfers between devices  56.7 us (29%)
  waiting for transfers between devices  55.5 us (28%)
  blocking collectives  48 us (24%)
  between operations  13.8 us (7%)
  matrix products  13.5 us (7%)
  other arithmetic  8.05 us (4%)
  local copies, waits for them, and re-layouts  2.02 us (1%)
    all_to_all x2, starting transfers between devices, sent_to_all(): lax.all_to_all(jnp.broadcast_to(value[None], (count, *value.shape)), axis...  51.1 us
    all_to_all x2, waiting for transfers between devices, sent_to_all(): lax.all_to_all(jnp.broadcast_to(value[None], (count, *value.shape)), axis...  33.6 us
    all_gather x1, waiting for transfers between devices, local(): segment = lax.all_gather(normed, 'tp', axis=0, tiled=True)  21.9 us
    all_to_all x1, blocking collectives, sent_to_all(): lax.all_to_all(jnp.broadcast_to(value[None], (count, *value.shape)), axis...  19.3 us
    all_gather x1, blocking collectives, rows_first(): whole, at, outs = (lax.all_gather(both, axis, axis=0, tiled=True), 0, [])  15.7 us
    all_to_all x1, blocking collectives, local(): lax.all_to_all(columns_part, 'tp', split_axis=0, concat_axis=1, tiled=True)  13 us
    ppermute x1, starting transfers between devices, with_halo(): lax.ppermute(tail, axis, [(i, (i + 1) % count) for i in range(ends)])  4.21 us
  transfers between devices with their start and end apart: 5, of which 2 were waited for; matrix products, arithmetic and copies ran while one was open for 6% of the time, Pallas kernels for 0%

commit v1 on v0

v1 whole, which is shorter than its diff:
```python
import functools

import jax
import jax.numpy as jnp
import numpy as np
from jax import lax
from jax.experimental import pallas as pl
from jax.experimental.pallas import tpu as pltpu
from jax.sharding import PartitionSpec as P

HEADS = 16
KV_HEADS = 8
HD = 64
GRID_W = 64
WIN = 128
REACH = 4
LANES = 128
COLS = 512

epsilon = 1e-06
rope_base = 10000.0
neg_large = -1e30
MESH = pl.DeviceIdType.MESH
f32 = jnp.float32
bf16 = jnp.bfloat16


def rope_tables(grid_rows):
    lane = np.arange(LANES)
    d = lane % HD
    freq = rope_base ** (-(d % 16) / 16.0)
    is_row = d < HD // 2
    sign = np.where(d % 32 < 16, -1.0, 1.0)
    is_key = lane < HD

    def table(count, own):
        angle = np.arange(count)[:, None] * freq[None, :]
        c = np.where(own, np.cos(angle), 0.0)
        s = np.where(own, np.sin(angle) * sign, 0.0)
        scale = HD**-0.5
        ck = np.where(is_key, c, 0.0)
        sk = np.where(is_key, s, 0.0)
        return np.concatenate([c * scale, s * scale, ck, sk], axis=1)

    rows = table(grid_rows, is_row)
    cols = table(GRID_W, ~is_row)
    cols[:, 2 * LANES : 3 * LANES] += np.where(is_key, 0.0, 1.0)
    return rows.astype(np.float32), cols.astype(np.float32)


def kernel(
    n_sp,
    n_tp,
    latent,
    context,
    cond,
    gain,
    shift_w,
    scale_w,
    gate_w,
    q_w,
    k_w,
    v_w,
    o_w,
    sink,
    row_tab,
    col_tab,
    out,
    rows,
    w,
    kw,
    vw,
    ow,
    mw,
    ctx_rows,
    cg,
    mpart,
    chain_l,
    chain_r,
    mtot,
    inv,
    a_vec,
    s_vec,
    g_vec,
    qrot,
    kv,
    ctx,
    att,
    ysend,
    yrecv,
    rt,
    ct,
    load_sem,
    m_send,
    m_recv,
    c_send,
    c_recv,
    x_send,
    x_recv,
    ag_send,
    ag_recv,
    fw_send,
    sib_send,
    sib_recv,
    h_send,
    h_recv,
    t_send,
    t_recv,
    tf_send,
    tsib_send,
    tsib_recv,
    y_send,
    y_recv,
):
    n_x = n_tp // 2
    z = lax.axis_index("sp")
    t = lax.axis_index("tp")
    x = t // 2
    c = t % 2
    xr = (x + 1) % n_x
    xl = (x + n_x - 1) % n_x
    xo = (x + 2) % n_x
    sib = x * 2 + (1 - c)
    t_r, t_l, t_o = xr * 2 + c, xl * 2 + c, xo * 2 + c
    fw_src = ((x + n_x - 1 + 2 * c) % n_x) * 2 + c
    fw_dst = ((x + 1 + n_x - 2 * c) % n_x) * 2 + c
    group = latent.shape[0]
    count = n_tp * group
    depth = latent.shape[1]
    chunks = group // 16
    width = shift_w.shape[1]
    per = width // LANES

    def up(k):
        return {"sp": (z + k) % n_sp}

    def down(k):
        return {"sp": (z + n_sp - k) % n_sp}

    def other(k):
        return {"tp": (t + k) % n_tp}

    started = []

    def send(src, dst, ss, rs, dev):
        copy = pltpu.make_async_remote_copy(
            src_ref=src, dst_ref=dst, send_sem=ss, recv_sem=rs, device_id=dev, device_id_type=MESH
        )
        copy.start()
        started.append(copy)

    def recv(dst, rs, dev):
        pltpu.make_async_remote_copy(
            src_ref=dst, dst_ref=dst, send_sem=rs, recv_sem=rs, device_id=dev, device_id_type=MESH
        ).wait_recv()

    barrier = pltpu.get_barrier_semaphore()
    for k in range(1, n_tp):
        pl.semaphore_signal(barrier, inc=1, device_id=other(k), device_id_type=MESH)
    for k in range(1, REACH + 1):
        pl.semaphore_signal(barrier, inc=1, device_id=up(k), device_id_type=MESH)
        pl.semaphore_signal(barrier, inc=1, device_id=down(k), device_id_type=MESH)

    grid_rows = count // GRID_W
    loads = {}

    def load(name, src, dst):
        copy = pltpu.make_async_copy(src, dst, load_sem.at[len(loads)])
        copy.start()
        loads[name] = copy

    load("m0", shift_w, mw.at[0])
    load("m1", scale_w, mw.at[1])
    load("m2", gate_w, mw.at[2])
    load("rows", latent, rows.at[t])
    load("kw", k_w, kw)
    load("vw", v_w, vw)
    load("ctx", context, ctx_rows)
    load("qw", q_w, w.at[:, pl.ds(0, LANES)])
    load("rt", row_tab.at[pl.ds(pl.multiple_of(z * grid_rows, 8), grid_rows)], rt)
    load("ct", col_tab, ct)
    load("ow", o_w, ow)

    cv = cond[...].astype(f32)
    lifted = jnp.broadcast_to((cv / (1.0 + jnp.exp(-cv))).astype(bf16), (16, cv.shape[1]))
    for i in range(3):
        loads["m%d" % i].wait()
        part = jnp.dot(lifted, mw[i], preferred_element_type=f32)
        for j in range(per):
            mpart[0, per * i + j : per * i + j + 1, :] = part[0:1, j * LANES : (j + 1) * LANES]
    mpart[0, 3 * per : 16, :] = jnp.zeros((16 - 3 * per, LANES), f32)

    loads["kw"].wait()
    loads["vw"].wait()
    for i in range(depth // COLS):
        part = pl.ds(i * COLS, COLS)
        w[part, LANES : 2 * LANES] = jnp.concatenate([kw[part, :], vw[part, :]], axis=1)
    loads["ctx"].wait()
    n_ctx = ctx_rows.shape[0]
    sq = jnp.zeros((n_ctx, LANES), f32)
    for i in range(depth // LANES):
        v = ctx_rows[:, i * LANES : (i + 1) * LANES].astype(f32)
        sq = sq + v * v
    cinv = lax.rsqrt(jnp.sum(sq, axis=1, keepdims=True) * (1.0 / depth) + epsilon)
    acc = jnp.zeros((n_ctx, LANES), f32)
    for i in range(depth // COLS):
        part = slice(i * COLS, (i + 1) * COLS)
        v = ctx_rows[:, part].astype(f32) * cinv * gain[:, part]
        acc = acc + jnp.dot(v.astype(bf16), w[part, LANES : 2 * LANES], preferred_element_type=f32)
    cg[0] = acc.astype(bf16)

    loads["rows"].wait()
    pl.semaphore_wait(barrier, n_tp - 1 + 2 * REACH)
    for k in range(1, REACH + 1):
        if k < REACH:
            send(mpart.at[0], mpart.at[k], m_send.at[k - 1], m_recv.at[k - 1], up(k))
        send(mpart.at[0], mpart.at[3 + k], m_send.at[2 + k], m_recv.at[2 + k], down(k))
    for q in range(chunks):
        piece = rows.at[t, pl.ds(16 * q, 16)]
        send(piece, piece, ag_send.at[0, q], ag_recv.at[0, q], {"tp": t_r})
        send(piece, piece, ag_send.at[1, q], ag_recv.at[1, q], {"tp": t_l})
    for q in range(chunks):
        piece = rows.at[t, pl.ds(16 * q, 16)]
        send(piece, piece, sib_send.at[0, q], sib_recv.at[0, q], {"tp": sib})
    half = n_sp // 2
    for k in range(1, REACH + 1):
        if k < REACH:
            send(cg.at[0], cg.at[k], c_send.at[k - 1], c_recv.at[k - 1], up(k))
        send(cg.at[0], cg.at[half + k - 1], c_send.at[2 + k], c_recv.at[2 + k], down(k))

    def row_stats(g):
        sq = jnp.zeros((group, LANES), f32)
        for i in range(depth // LANES):
            v = rows[g, :, i * LANES : (i + 1) * LANES].astype(f32)
            sq = sq + v * v
        r = lax.rsqrt(jnp.sum(sq, axis=1, keepdims=True) * (1.0 / depth) + epsilon)
        inv[g] = jnp.broadcast_to(r, (group, LANES))

    def chunk_step(q, relay):
        piece_l = rows.at[t_l, pl.ds(16 * q, 16)]
        piece_r = rows.at[t_r, pl.ds(16 * q, 16)]
        recv(piece_l, ag_recv.at[0, q], {"tp": t_l})
        recv(piece_r, ag_recv.at[1, q], {"tp": t_r})
        if relay:
            chunk_relay(q)
        send(piece_l, piece_l, sib_send.at[1, q], sib_recv.at[1, q], {"tp": sib})
        send(piece_r, piece_r, sib_send.at[2, q], sib_recv.at[2, q], {"tp": sib})

    def chunk_relay(q):
        piece = rows.at[fw_src, pl.ds(16 * q, 16)]
        send(piece, piece, fw_send.at[q], ag_recv.at[2, q], {"tp": fw_dst})

    stages = half // REACH

    def mod_step(s):
        if s == 0:
            for k in range(1, REACH + 1):
                if k < REACH:
                    recv(mpart.at[k], m_recv.at[k - 1], down(k))
                recv(mpart.at[3 + k], m_recv.at[2 + k], up(k))
            chain_l[0] = (mpart[0] + mpart[1]) + (mpart[2] + mpart[3])
            chain_r[0] = (mpart[4] + mpart[5]) + (mpart[6] + mpart[7])
        else:
            recv(chain_l.at[s], m_recv.at[5 + 2 * s], down(REACH))
            recv(chain_r.at[s], m_recv.at[6 + 2 * s], up(REACH))
        if s + 1 < stages:
            send(chain_l.at[s], chain_l.at[s + 1], m_send.at[7 + 2 * s], m_recv.at[7 + 2 * s], up(REACH))
            send(chain_r.at[s], chain_r.at[s + 1], m_send.at[8 + 2 * s], m_recv.at[8 + 2 * s], down(REACH))

    def ctx_step(s):
        if s == 0:
            for k in range(1, REACH + 1):
                if k < REACH:
                    recv(cg.at[k], c_recv.at[k - 1], down(k))
                recv(cg.at[half + k - 1], c_recv.at[2 + k], up(k))
        else:
            recv(cg.at[pl.ds(REACH * s, REACH)], c_recv.at[5 + 2 * s], down(REACH))
            recv(cg.at[pl.ds(half + REACH * s, REACH)], c_recv.at[6 + 2 * s], up(REACH))
        if s + 1 < stages:
            for base, j, dev in ((0, 7, up(REACH)), (half, 8, down(REACH))):
                send(
                    cg.at[pl.ds(base + REACH * s, REACH)],
                    cg.at[pl.ds(base + REACH * (s + 1), REACH)],
                    c_send.at[j + 2 * s],
                    c_recv.at[j + 2 * s],
                    dev,
                )

    row_stats(t)
    mod_step(0)
    chunk_step(0, True)
    ctx_step(0)
    chunk_step(1, True)
    mod_step(1)
    ctx_step(1)
    chunk_step(2, True)
    mod_step(2)
    ctx_step(2)
    chunk_step(3, False)
    row_stats(t_l)
    row_stats(t_r)
    mod_step(3)

    mtot[t] = ((chain_l[0] + chain_l[1]) + (chain_l[2] + chain_l[3])) + (
        (chain_r[0] + chain_r[1]) + (chain_r[2] + chain_r[3])
    )
    for k in range(1, n_tp):
        send(mtot.at[t], mtot.at[t], x_send.at[k - 1], x_recv.at[k - 1], other(k))
    chunk_relay(3)
    ctx_step(3)
    for j in range(n_sp):
        ctx[pl.ds(j * n_ctx, n_ctx), :] = cg[j]

    for name in ("rt", "ct", "qw", "ow"):
        loads[name].wait()
    for q in range(chunks):
        for role, src in ((0, sib), (1, xl * 2 + 1 - c), (2, xr * 2 + 1 - c)):
            recv(rows.at[src, pl.ds(16 * q, 16)], sib_recv.at[role, q], {"tp": sib})
    row_stats(sib)
    row_stats(xl * 2 + 1 - c)
    row_stats(xr * 2 + 1 - c)
    for q in range(chunks):
        piece = rows.at[t_o, pl.ds(16 * q, 16)]
        recv(piece, ag_recv.at[2, q], {"tp": t_o})
        send(piece, piece, sib_send.at[3, q], sib_recv.at[3, q], {"tp": sib})
    row_stats(t_o)
    for k in range(1, n_tp):
        src = (t + n_tp - k) % n_tp
        recv(mtot.at[src], x_recv.at[k - 1], {"tp": src})
    for j in range(n_tp):
        for i in range(per):
            part = slice(j * width + i * LANES, j * width + (i + 1) * LANES)
            s_vec[:, part] = mtot[j, i : i + 1, :]
            a_vec[:, part] = gain[:, part] * (1.0 + mtot[j, per + i : per + i + 1, :])
            g_vec[:, part] = mtot[j, 2 * per + i : 2 * per + i + 1, :]
    for q in range(chunks):
        src = xo * 2 + 1 - c
        recv(rows.at[src, pl.ds(16 * q, 16)], sib_recv.at[3, q], {"tp": sib})
    row_stats(xo * 2 + 1 - c)

    lane = lax.broadcasted_iota(jnp.int32, (1, LANES), 1)
    first = lane % 32 < 16

    def swapped(v):
        return jnp.where(first, pltpu.roll(v, LANES - 16, 1), pltpu.roll(v, 16, 1))

    def project(gs):
        acc = jnp.zeros((len(gs) * group, 2 * LANES), f32)
        for i in range(depth // COLS):
            part = slice(i * COLS, (i + 1) * COLS)
            a = a_vec[:, part]
            s = s_vec[:, part]
            tiles = []
            for g in gs:
                r = jnp.concatenate([inv[g]] * (COLS // LANES), axis=1)
                tiles.append((rows[g, :, part].astype(f32) * r * a + s).astype(bf16))
            acc = acc + jnp.dot(jnp.concatenate(tiles, axis=0), w[part, :], preferred_element_type=f32)
        for n, g in enumerate(gs):
            fac = rt[g : g + 1, :] + ct[...]
            vq = acc[n * group : (n + 1) * group, :LANES]
            vk = acc[n * group : (n + 1) * group, LANES:]
            q2 = vq * fac[:, :LANES] + swapped(vq) * fac[:, LANES : 2 * LANES]
            k2 = vk * fac[:, 2 * LANES : 3 * LANES] + swapped(vk) * fac[:, 3 * LANES :]
            qrot[g * group : (g + 1) * group, :] = q2.astype(bf16)
            kv[WIN + g * group : WIN + (g + 1) * group, :] = k2.astype(bf16)

    project((0, 1, n_tp - 2, n_tp - 1))
    send(kv.at[pl.ds(WIN, WIN)], kv.at[pl.ds(WIN + count, WIN)], h_send.at[0], h_recv.at[0], down(1))
    send(kv.at[pl.ds(count, WIN)], kv.at[pl.ds(0, WIN)], h_send.at[1], h_recv.at[1], up(1))
    project(tuple(range(2, n_tp - 2)))

    rows2 = 2 * WIN
    qi = lax.broadcasted_iota(jnp.int32, (rows2, WIN), 0) % WIN
    ki = lax.broadcasted_iota(jnp.int32, (rows2, WIN), 1)
    head1 = lax.broadcasted_iota(jnp.int32, (rows2, 1), 0) >= WIN
    sink_col = jnp.where(head1, sink[1], sink[0])
    is_key = lane < HD
    contract = (((1,), (1,)), ((), ()))
    blocks = count // WIN

    def attend(b):
        qb = qrot[b * WIN : (b + 1) * WIN, :].astype(f32)
        q0 = jnp.where(is_key, qb, 0.0).astype(bf16)
        q1 = jnp.where(is_key, pltpu.roll(qb, HD, 1), 0.0).astype(bf16)
        qq = jnp.concatenate([q0, q1], axis=0)
        band = kv[b * WIN : (b + 3) * WIN, :]
        whole = ctx[...]
        s_band = lax.dot_general(qq, band, contract, preferred_element_type=f32)
        s_ctx = lax.dot_general(qq, whole, contract, preferred_element_type=f32)
        left = ki >= qi
        right = ki <= qi
        if b == 0:
            left = left & (z > 0)
        if b == blocks - 1:
            right = right & (z < n_sp - 1)
        s0 = jnp.where(left, s_band[:, :WIN], neg_large)
        s1 = s_band[:, WIN : 2 * WIN]
        s2 = jnp.where(right, s_band[:, 2 * WIN :], neg_large)
        top = jnp.maximum(jnp.maximum(s0, s1), s2)
        for i in range(whole.shape[0] // LANES):
            top = jnp.maximum(top, s_ctx[:, i * LANES : (i + 1) * LANES])
        m = jnp.maximum(jnp.max(top, axis=1, keepdims=True), sink_col)
        e0 = jnp.exp(s0 - m)
        e1 = jnp.exp(s1 - m)
        e2 = jnp.exp(s2 - m)
        ec = jnp.exp(s_ctx - m)
        tot = e0 + e1 + e2
        for i in range(whole.shape[0] // LANES):
            tot = tot + ec[:, i * LANES : (i + 1) * LANES]
        den = jnp.sum(tot, axis=1, keepdims=True) + jnp.exp(sink_col - m)
        r = 1.0 / den
        p_band = jnp.concatenate([e0, e1, e2], axis=1) * r
        o = jnp.dot(p_band.astype(bf16), band, preferred_element_type=f32) + jnp.dot(
            (ec * r).astype(bf16), whole, preferred_element_type=f32
        )
        res = jnp.where(is_key, pltpu.roll(o[:WIN], HD, 1), o[WIN:]).astype(bf16)
        att[t, b * WIN : (b + 1) * WIN, :] = res

    def att_piece(who, b):
        return att.at[who, pl.ds(b * WIN, WIN)]

    def att_send(b):
        piece = att_piece(t, b)
        send(piece, piece, t_send.at[0, b], t_recv.at[0, b], {"tp": t_r})
        send(piece, piece, t_send.at[1, b], t_recv.at[1, b], {"tp": t_l})
        send(piece, piece, tsib_send.at[0, b], tsib_recv.at[0, b], {"tp": sib})

    def att_near(b):
        piece_l, piece_r = att_piece(t_l, b), att_piece(t_r, b)
        recv(piece_l, t_recv.at[0, b], {"tp": t_l})
        recv(piece_r, t_recv.at[1, b], {"tp": t_r})
        piece = att_piece(fw_src, b)
        send(piece, piece, tf_send.at[b], t_recv.at[2, b], {"tp": fw_dst})
        send(piece_l, piece_l, tsib_send.at[1, b], tsib_recv.at[1, b], {"tp": sib})
        send(piece_r, piece_r, tsib_send.at[2, b], tsib_recv.at[2, b], {"tp": sib})

    def att_far(b):
        piece = att_piece(t_o, b)
        recv(piece, t_recv.at[2, b], {"tp": t_o})
        send(piece, piece, tsib_send.at[3, b], tsib_recv.at[3, b], {"tp": sib})

    order = [*range(1, blocks - 1), 0, blocks - 1]
    for n, b in enumerate(order):
        if n == blocks - 2:
            recv(kv.at[pl.ds(WIN + count, WIN)], h_recv.at[0], up(1))
            recv(kv.at[pl.ds(0, WIN)], h_recv.at[1], down(1))
        attend(b)
        att_send(b)
        if n >= 1:
            att_near(order[n - 1])
        if n >= 2:
            att_far(order[n - 2])
    att_near(order[-1])
    att_far(order[-2])
    att_far(order[-1])
    for b in order:
        for role, xx in ((0, x), (1, xl), (2, xr), (3, xo)):
            recv(att_piece(xx * 2 + 1 - c, b), tsib_recv.at[role, b], {"tp": sib})

    here = pl.ds(pl.multiple_of(t * width, LANES), width)
    for n, xx in enumerate((xo, xr, xl, x)):
        part = pl.ds(pl.multiple_of(xx * WIN, WIN), WIN)
        y = jnp.zeros((WIN, width), f32)
        for i in range(n_x):
            lhs = jnp.concatenate([att[2 * i, part, :], att[2 * i + 1, part, :]], axis=1)
            y = y + jnp.dot(lhs, ow[2 * i * LANES : 2 * (i + 1) * LANES, :], preferred_element_type=f32)
        ysend[2 * n] = y[:group].astype(bf16)
        ysend[2 * n + 1] = y[group:].astype(bf16)
        if n < 3:
            for k in range(2):
                send(ysend.at[2 * n + k], yrecv.at[:, here], y_send.at[2 * n + k], y_recv.at[2 * n + c], {"tp": xx * 2 + k})
        else:
            send(ysend.at[2 * n + 1 - c], yrecv.at[:, here], y_send.at[6], y_recv.at[6], {"tp": sib})
            yrecv[:, here] = ysend[2 * n + c]
    for n, xx in enumerate((xo, xl, xr)):
        for k in range(2):
            cols = pl.ds(pl.multiple_of((xx * 2 + k) * width, LANES), width)
            recv(yrecv.at[:, cols], y_recv.at[2 * n + k], {"tp": xx * 2 + k})
    recv(yrecv.at[:, pl.ds(pl.multiple_of(sib * width, LANES), width)], y_recv.at[6], {"tp": sib})
    for i in range(depth // COLS):
        part = slice(i * COLS, (i + 1) * COLS)
        out[:, part] = (
            rows[t, :, part].astype(f32) + g_vec[:, part] * yrecv[:, part].astype(f32)
        ).astype(bf16)
    for copy in started:
        copy.wait_send()


def local(n_sp, n_tp, latent, context, conditioning, norm_gain, *rest):
    shift_w, scale_w, gate_w, q_w, k_w, v_w, o_w, sink = rest
    group, depth = latent.shape
    n_ctx = context.shape[0]
    count = n_tp * group
    width = shift_w.shape[1]
    blocks = count // WIN
    chunks = group // 16
    row_tab, col_tab = rope_tables(n_sp * count // GRID_W)
    any_space = pl.BlockSpec(memory_space=pl.ANY)
    vmem = pl.BlockSpec(memory_space=pltpu.VMEM)
    dma = pltpu.SemaphoreType.DMA
    return pl.pallas_call(
        functools.partial(kernel, n_sp, n_tp),
        out_shape=jax.ShapeDtypeStruct((group, depth), bf16),
        in_specs=[any_space, any_space, vmem, vmem]
        + [any_space] * 7
        + [pl.BlockSpec(memory_space=pltpu.SMEM), any_space, any_space],
        out_specs=vmem,
        scratch_shapes=[
            pltpu.VMEM((n_tp, group, depth), bf16),
            pltpu.VMEM((depth, 2 * LANES), bf16),
            pltpu.VMEM(k_w.shape, bf16),
            pltpu.VMEM(v_w.shape, bf16),
            pltpu.VMEM(o_w.shape, bf16),
            pltpu.VMEM((3, *shift_w.shape), bf16),
            pltpu.VMEM((n_ctx, depth), bf16),
            pltpu.VMEM((n_sp, n_ctx, LANES), bf16),
            pltpu.VMEM((2 * REACH, 16, LANES), f32),
            pltpu.VMEM((n_sp // 2 // REACH, 16, LANES), f32),
            pltpu.VMEM((n_sp // 2 // REACH, 16, LANES), f32),
            pltpu.VMEM((n_tp, 16, LANES), f32),
            pltpu.VMEM((n_tp, group, LANES), f32),
            pltpu.VMEM((1, depth), f32),
            pltpu.VMEM((1, depth), f32),
            pltpu.VMEM((1, depth), f32),
            pltpu.VMEM((count, LANES), bf16),
            pltpu.VMEM((count + 2 * WIN, LANES), bf16),
            pltpu.VMEM((n_sp * n_ctx, LANES), bf16),
            pltpu.VMEM((n_tp, count, LANES), bf16),
            pltpu.VMEM((n_tp, group, width), bf16),
            pltpu.VMEM((group, depth), bf16),
            pltpu.VMEM((count // GRID_W, 4 * LANES), f32),
            pltpu.VMEM((GRID_W, 4 * LANES), f32),
            dma((16,)),
            dma((16,)),
            dma((16,)),
            dma((16,)),
            dma((16,)),
            dma((n_tp,)),
            dma((n_tp,)),
            dma((2, chunks)),
            dma((3, chunks)),
            dma((chunks,)),
            dma((4, chunks)),
            dma((4, chunks)),
            dma((2,)),
            dma((2,)),
            dma((2, blocks)),
            dma((3, blocks)),
            dma((blocks,)),
            dma((4, blocks)),
            dma((4, blocks)),
            dma((8,)),
            dma((8,)),
        ],
        compiler_params=pltpu.CompilerParams(
            collective_id=0, has_side_effects=True, vmem_limit_bytes=56 * 1024 * 1024
        ),
    )(
        latent,
        context,
        conditioning.reshape(1, -1),
        norm_gain.reshape(1, -1),
        shift_w,
        scale_w,
        gate_w,
        q_w,
        k_w,
        v_w,
        o_w,
        sink,
        jnp.asarray(row_tab),
        jnp.asarray(col_tab),
    )


def solution(mesh):
    in_specs = (
        P(("grp", "sp", "tp"), None),
        P(("grp", "sp"), None),
        P(("grp", "sp")),
        P(),
        P("sp", "tp"),
        P("sp", "tp"),
        P("sp", "tp"),
        P(None, "tp"),
        P(None, "tp"),
        P(None, "tp"),
        P(None, "tp"),
        P("tp"),
    )
    return jax.shard_map(
        functools.partial(local, mesh.shape["sp"], mesh.shape["tp"]),
        mesh=mesh,
        in_specs=in_specs,
        out_specs=P(("grp", "sp", "tp"), None),
        check_vma=False,
    )
```

time: 198 us -> 108 us (0.55)
  Pallas kernels: 0 us -> 102 us
  starting transfers between devices: 56.7 us -> 0 us
  waiting for transfers between devices: 55.5 us -> 0 us
  blocking collectives: 48 us -> 0 us
  between operations: 13.8 us -> 0.01 us
  matrix products: 13.5 us -> 0 us
  other arithmetic: 8.05 us -> 0 us
  local copies, waits for them, and re-layouts: 2.02 us -> 5.68 us
    pallas_call x0 -> x1, Pallas kernels: none -> 102 us  [local(): pl.pallas_call(functools.partial(kernel, n_sp, n_tp), out_shape=jax.Shape...]
    all_to_all x2 -> x0, starting transfers between devices: 51.1 us -> none  [sent_to_all(): lax.all_to_all(jnp.broadcast_to(value[None], (count, *value.shape)), axis...]
    all_to_all x2 -> x0, waiting for transfers between devices: 33.6 us -> none  [sent_to_all(): lax.all_to_all(jnp.broadcast_to(value[None], (count, *value.shape)), axis...]
    all_to_all x2 -> x0, blocking collectives: 32.3 us -> none  [the longest x1 19.3 us: sent_to_all(): lax.all_to_all(jnp.broadcast_to(value[None], (count, *value.shape)), axis...]
    all_gather x1 -> x0, waiting for transfers between devices: 21.9 us -> none  [local(): segment = lax.all_gather(normed, 'tp', axis=0, tiled=True)]
    all_gather x1 -> x0, blocking collectives: 15.7 us -> none  [rows_first(): whole, at, outs = (lax.all_gather(both, axis, axis=0, tiled=True), 0, [])]
    dot_general x13 -> x0, matrix products: 13.5 us -> none  [the longest x1 3.72 us: local(): jnp.dot(segment, key_weight, preferred_element_type=jnp.float32)]
    ppermute x2 -> x0, starting transfers between devices: 5.52 us -> none  [the longest x1 4.21 us: with_halo(): lax.ppermute(tail, axis, [(i, (i + 1) % count) for i in range(ends)])]
  transfers between devices with their start and end apart: 5 -> 0, of which waited for: 2 -> 0; matrix products, arithmetic and copies ran while one was open for 6% -> 0% of each run, Pallas kernels for 0% -> 0%
where the time goes in v1:
time: 108 us; the launch traced here: 107 us
  Pallas kernels  102 us (94%)
  local copies, waits for them, and re-layouts  5.68 us (5%)
    pallas_call x1, Pallas kernels, local(): pl.pallas_call(functools.partial(kernel, n_sp, n_tp), out_shape=jax.Shape...  102 us
    unnamed x5, local copies, waits for them, and re-layouts  5.68 us

profile of v1, /device:TPU:33, one launch (start us, length us, event | category | flops | bytes accessed | tf_op | source)
XLA Modules:
  0.0 107.5 jit_solution(277730623518583285)
XLA Ops:
  0.0 0.0 copy-start
  0.0 2.4 %copy.15.k_w = bf16[4096,64]{1,0:T(8,128)(2,1)} copy(bf16[4096,64]{0,1:T(8,128)(2,1)} %param.22) | data formatting | bytes 1048576 | tf_op args[8]
  2.4 0.0 copy-done
  2.4 1.4 %copy.16.v_w = bf16[4096,64]{1,0:T(8,128)(2,1)} copy(bf16[4096,64]{0,1:T(8,128)(2,1)S(1)} %copy-done) | data formatting | bytes 1048576 | tf_op args[9]
  3.8 101.8 %shard_map.136 = bf16[64,4096]{1,0:T(8,128)(2,1)} custom-call(bf16[64,4096]{1,0:T(8,128)(2,1)} %latent.1, bf16[24,4096]{1,0:T(8,128)(2,1)} %context.1, bf16[1,128]{1,0:T(2,128)(2,1)} %bitcast.3, f32[1,4096]{1,0:T(1,128)} %bitcast.2, bf16[128,512]{1,0:T(8,128)(2,1)} %shift_w.1, bf16[128,512]{1,0:T(8,128)(2,1)} %scale_w.1, bf16[128,512]{1,0:T(8,128)(2,1)} %gate_w.1, ...), custom_call_target="tpu_custom_call" | custom-call | tf_op jit(solution)/shard_map/pallas_call | solution.py:501
  105.6 1.9 %copy.18 = bf16[64,4096]{1,0:T(8,128)(2,1)} copy(bf16[64,4096]{1,0:T(8,128)(2,1)} %shard_map.136) | data formatting | bytes 1048576
Async XLA Ops:
  0.0 2.4 %copy-start = (bf16[4096,64]{0,1:T(8,128)(2,1)S(1)}, bf16[4096,64]{0,1:T(8,128)(2,1)}, u32[]{:S(2)}) copy-start(bf16[4096,64]{0,1:T(8,128)(2,1)} %param.23) | copy-start | bytes 1572868

commit v2 on v1

v2 whole, which is shorter than its diff:
```python
import functools

import jax
import jax.numpy as jnp
import numpy as np
from jax import lax
from jax.experimental import pallas as pl
from jax.experimental.pallas import tpu as pltpu
from jax.sharding import PartitionSpec as P

HEADS = 16
KV_HEADS = 8
HD = 64
GRID_W = 64
WIN = 128
LANES = 128
COLS = 512

epsilon = 1e-06
rope_base = 10000.0
neg_large = -1e30
MESH = pl.DeviceIdType.MESH
f32 = jnp.float32
bf16 = jnp.bfloat16


def rope_tables(grid_rows):
    lane = np.arange(LANES)
    d = lane % HD
    freq = rope_base ** (-(d % 16) / 16.0)
    is_row = d < HD // 2
    sign = np.where(d % 32 < 16, -1.0, 1.0)
    is_key = lane < HD

    def table(count, own):
        angle = np.arange(count)[:, None] * freq[None, :]
        c = np.where(own, np.cos(angle), 0.0)
        s = np.where(own, np.sin(angle) * sign, 0.0)
        scale = HD**-0.5
        ck = np.where(is_key, c, 0.0)
        sk = np.where(is_key, s, 0.0)
        return np.concatenate([c * scale, s * scale, ck, sk], axis=1)

    rows = table(grid_rows, is_row)
    cols = table(GRID_W, ~is_row)
    cols[:, 2 * LANES : 3 * LANES] += np.where(is_key, 0.0, 1.0)
    return rows.astype(np.float32), cols.astype(np.float32)


def kernel(
    n_sp,
    n_tp,
    latent,
    context,
    cond_in,
    gain_in,
    shift_w,
    scale_w,
    gate_w,
    q_w,
    k_t,
    v_t,
    o_w,
    sink_in,
    row_tab,
    col_tab,
    out,
    rows,
    w,
    kvt,
    ow,
    mw,
    ctx_rows,
    cg,
    cown,
    mpair,
    mall,
    msum,
    mt,
    inv,
    a_vec,
    s_vec,
    g_vec,
    qrot,
    kv,
    ctx,
    att,
    ysend,
    yrecv,
    rt,
    ct,
    cond,
    gain,
    sink,
    hello,
    load_sem,
    pair_send,
    pair_recv,
    m_send,
    m_recv,
    tot_send,
    tot_recv,
    c_send,
    c_recv,
    ag_send,
    ag_recv,
    sib_send,
    sib_recv,
    x_send,
    x_recv,
    xs_send,
    xs_recv,
    h_send,
    h_recv,
    t_send,
    t_recv,
    tsib_send,
    tsib_recv,
    y_send,
    y_recv,
):
    n_x = n_tp // 2
    z = lax.axis_index("sp")
    t = lax.axis_index("tp")
    x = t // 2
    c = t % 2
    xr = (x + 1) % n_x
    xl = (x + n_x - 1) % n_x
    xo = (x + 2) % n_x
    sib = x * 2 + (1 - c)
    t_r, t_l, t_o = xr * 2 + c, xl * 2 + c, xo * 2 + c
    group = latent.shape[0]
    count = n_tp * group
    depth = latent.shape[1]
    chunks = group // 16
    width = shift_w.shape[1]
    per = width // LANES

    late = (z == 0) & (x == 0)
    center = 1

    started = []

    def send(src, dst, ss, rs, dev, keep=True):
        copy = pltpu.make_async_remote_copy(
            src_ref=src, dst_ref=dst, send_sem=ss, recv_sem=rs, device_id=dev, device_id_type=MESH
        )
        copy.start()
        if keep:
            started.append(copy)

    def recv(dst, rs, dev):
        pltpu.make_async_remote_copy(
            src_ref=dst, dst_ref=dst, send_sem=rs, recv_sem=rs, device_id=dev, device_id_type=MESH
        ).wait_recv()

    def sent(src, ss, dev):
        pltpu.make_async_remote_copy(
            src_ref=src, dst_ref=src, send_sem=ss, recv_sem=ss, device_id=dev, device_id_type=MESH
        ).wait_send()

    def each(lo, hi, body):
        def step(i, carry):
            body(i)
            return carry

        lax.fori_loop(lo, hi, step, 0)

    barrier = pltpu.get_barrier_semaphore()

    def greet(dev):
        pl.semaphore_signal(barrier, inc=1, device_id=dev, device_id_type=MESH)

    @pl.when(c == 1)
    def _():
        for who in (sib, t_r, t_l, t_o):
            greet({"tp": who})

    @pl.when(c == 0)
    def _():
        each(z + 1, n_sp, lambda i: greet({"sp": i}))

    @pl.when((c == 0) & (z == center))
    def _():
        each(0, center, lambda i: greet({"sp": i}))

    grid_rows = count // GRID_W
    loads = {}

    def load(name, src, dst):
        copy = pltpu.make_async_copy(src, dst, load_sem.at[len(loads)])
        copy.start()
        loads[name] = copy

    load("cond", cond_in, cond)
    load("m0", shift_w, mw.at[0])
    load("m1", scale_w, mw.at[1])
    load("m2", gate_w, mw.at[2])
    load("rows", latent, rows.at[t])
    load("gain", gain_in, gain)
    load("kw", k_t, kvt.at[pl.ds(0, HD)])
    load("vw", v_t, kvt.at[pl.ds(HD, HD)])
    load("ctx", context, ctx_rows)
    load("qw", q_w, w.at[:, pl.ds(0, LANES)])
    load("rt", row_tab.at[pl.ds(pl.multiple_of(z * grid_rows, 8), grid_rows)], rt)
    load("ct", col_tab, ct)
    load("sink", sink_in, sink)
    load("ow", o_w, ow)

    def contact():
        pl.semaphore_wait(barrier, c * 3 + (1 - c) * (1 + z + jnp.where(z < center, 1, 0)))

    def modulation():
        loads["cond"].wait()
        cv = cond[...].astype(f32)
        lifted = jnp.broadcast_to((cv / (1.0 + jnp.exp(-cv))).astype(bf16), (16, cv.shape[1]))
        for i in range(3):
            loads["m%d" % i].wait()
            part = jnp.dot(lifted, mw[i], preferred_element_type=f32)
            for j in range(per):
                mpair[c, per * i + j : per * i + j + 1, :] = part[0:1, j * LANES : (j + 1) * LANES]
        mpair[c, 3 * per : 16, :] = jnp.zeros((16 - 3 * per, LANES), f32)

    n_ctx = ctx_rows.shape[0]

    def own_context():
        for name in ("kw", "vw", "gain", "ctx"):
            loads[name].wait()
        for i in range(depth // COLS):
            w[i * COLS : (i + 1) * COLS, LANES : 2 * LANES] = kvt[:, i * COLS : (i + 1) * COLS].T
        sq = jnp.zeros((n_ctx, LANES), f32)
        for i in range(depth // LANES):
            v = ctx_rows[:, i * LANES : (i + 1) * LANES].astype(f32)
            sq = sq + v * v
        cinv = lax.rsqrt(jnp.sum(sq, axis=1, keepdims=True) * (1.0 / depth) + epsilon)
        acc = jnp.zeros((n_ctx, LANES), f32)
        for i in range(depth // COLS):
            part = slice(i * COLS, (i + 1) * COLS)
            v = ctx_rows[:, part].astype(f32) * cinv * gain[:, part]
            acc = acc + jnp.dot(v.astype(bf16), w[part, LANES : 2 * LANES], preferred_element_type=f32)
        cown[...] = acc.astype(bf16)

    def row_stats(g):
        sq = jnp.zeros((group, LANES), f32)
        for i in range(depth // LANES):
            v = rows[g, :, i * LANES : (i + 1) * LANES].astype(f32)
            sq = sq + v * v
        r = lax.rsqrt(jnp.sum(sq, axis=1, keepdims=True) * (1.0 / depth) + epsilon)
        inv[g] = jnp.broadcast_to(r, (group, LANES))

    @pl.when(z == 0)
    def _():
        kv[:WIN, :] = jnp.zeros((WIN, LANES), bf16)

    @pl.when(z == n_sp - 1)
    def _():
        kv[WIN + count :, :] = jnp.zeros((WIN, LANES), bf16)

    def piece(g, q):
        return rows.at[g, pl.ds(16 * q, 16)]

    zero_l, zero_r, zero_o = t_l - c, t_r - c, t_o - c

    def meet():
        pl.semaphore_wait(hello, 1)
        send(mpair.at[1], mpair.at[1], pair_send.at[0], pair_recv.at[0], {"tp": sib}, False)

    def hand_context():
        send(cown, cg.at[z, 1], pair_send.at[1], pair_recv.at[1], {"tp": sib}, False)

    def sibling_rows():
        recv(rows.at[sib], sib_recv.at[sib], {"tp": sib})
        for q in range(chunks):
            send(piece(sib, q), piece(sib, q), ag_send.at[2, q], ag_recv.at[2, q], {"tp": t_r}, False)
            send(piece(sib, q), piece(sib, q), ag_send.at[3, q], ag_recv.at[3, q], {"tp": t_l}, False)

    def hand(groups):
        for g in groups:
            send(rows.at[g], rows.at[g], sib_send.at[g], sib_recv.at[g], {"tp": sib}, False)

    @pl.when(c == 1)
    def _():
        loads["rows"].wait()
        contact()
        for q in range(chunks):
            send(piece(t, q), piece(t, q), ag_send.at[0, q], ag_recv.at[0, q], {"tp": t_r}, False)
            send(piece(t, q), piece(t, q), ag_send.at[1, q], ag_recv.at[1, q], {"tp": t_l}, False)
        modulation()
        pl.when(~late)(meet)
        own_context()
        pl.when(~late)(hand_context)
        pl.when(~late)(sibling_rows)
        for q in range(chunks):
            recv(piece(t_r, q), ag_recv.at[1, q], {"tp": t_r})
            send(piece(t_r, q), piece(t_r, q), ag_send.at[4, q], ag_recv.at[4, q], {"tp": t_l}, False)
        for q in range(chunks):
            recv(piece(t_l, q), ag_recv.at[0, q], {"tp": t_l})
        pl.when(~late)(functools.partial(hand, (t, t_r, t_l)))
        row_stats(t)
        row_stats(t_l)
        row_stats(t_r)
        for q in range(chunks):
            recv(piece(zero_l, q), ag_recv.at[2, q], {"tp": t_l})
            send(piece(zero_l, q), piece(zero_l, q), ag_send.at[5, q], ag_recv.at[5, q], {"tp": t_r}, False)
        for q in range(chunks):
            recv(piece(zero_r, q), ag_recv.at[3, q], {"tp": t_r})
        pl.when(~late)(functools.partial(hand, (zero_l, zero_r)))
        row_stats(zero_l)
        row_stats(zero_r)
        for q in range(chunks):
            recv(piece(t_o, q), ag_recv.at[4, q], {"tp": t_r})
        pl.when(~late)(functools.partial(hand, (t_o,)))
        row_stats(t_o)
        for q in range(chunks):
            recv(piece(zero_o, q), ag_recv.at[5, q], {"tp": t_l})
        pl.when(~late)(functools.partial(hand, (zero_o,)))
        row_stats(zero_o)

        @pl.when(late)
        def _():
            meet()
            hand_context()
            sibling_rows()
            hand((t, t_r, t_l, zero_l, zero_r, t_o, zero_o))

        row_stats(sib)
        recv(mt.at[x], xs_recv.at[x], {"tp": sib})
        for n, (who, xx) in enumerate(((t_r, xr), (t_l, xl), (t_o, xo))):
            send(mt.at[x], mt.at[x], x_send.at[n], x_recv.at[x], {"tp": who}, False)
        for who, xx in ((t_r, xr), (t_l, xl), (t_o, xo)):
            recv(mt.at[xx], x_recv.at[xx], {"tp": who})
            send(mt.at[xx], mt.at[xx], xs_send.at[xx], xs_recv.at[xx], {"tp": sib}, False)
        recv(cg.at[:, 1], pair_recv.at[2], {"tp": sib})

    @pl.when(c == 0)
    def _():
        modulation()
        loads["rows"].wait()
        contact()
        pl.semaphore_signal(hello, inc=1, device_id={"tp": sib}, device_id_type=MESH)
        send(rows.at[t], rows.at[t], sib_send.at[t], sib_recv.at[t], {"tp": sib}, False)
        recv(mpair.at[1], pair_recv.at[0], {"tp": sib})

        @pl.when(z != center)
        def _():
            send(mpair, mall.at[z], m_send.at[0], m_recv.at[z], {"sp": center}, False)

        @pl.when(z == center)
        def _():
            mall[center] = mpair[...]

        own_context()
        cg[z, 0] = cown[...]
        row_stats(t)
        recv(cg.at[z, 1], pair_recv.at[1], {"tp": sib})

        def give(i):
            send(cg.at[z], cg.at[z], c_send.at[i], c_recv.at[z], {"sp": i}, False)

        def answer(i):
            recv(cg.at[i], c_recv.at[i], {"sp": i})
            give(i)

        each(0, z, give)
        each(z + 1, n_sp, answer)

        @pl.when(z == center)
        def _():
            def take(i):
                @pl.when(i != center)
                def _():
                    recv(mall.at[i], m_recv.at[i], {"sp": i})

            each(0, n_sp, take)
            tot = mall[0]
            for i in range(1, n_sp):
                tot = tot + mall[i]
            msum[...] = tot

            def tell(i):
                @pl.when(i != center)
                def _():
                    send(msum, mt.at[x], tot_send.at[i], tot_recv, {"sp": i}, False)

            each(0, n_sp, tell)
            mt[x] = tot

        @pl.when(z != center)
        def _():
            recv(mt.at[x], tot_recv, {"sp": center})

        send(mt.at[x], mt.at[x], xs_send.at[x], xs_recv.at[x], {"tp": sib}, False)
        each(0, z, lambda i: recv(cg.at[i], c_recv.at[i], {"sp": i}))
        send(cg.at[:, 1], cg.at[:, 1], pair_send.at[2], pair_recv.at[2], {"tp": sib}, False)
        for g in (sib, t_r + 1, t_l + 1, t_r, t_l, t_o + 1, t_o):
            recv(rows.at[g], sib_recv.at[g], {"tp": sib})
            row_stats(g)
        for xx in (xr, xl, xo):
            recv(mt.at[xx], xs_recv.at[xx], {"tp": sib})

    for j in range(n_sp):
        ctx[pl.ds(j * n_ctx, n_ctx), :] = cg[j, c]
    for j in range(n_tp):
        for i in range(per):
            part = slice(j * width + i * LANES, j * width + (i + 1) * LANES)
            s_vec[:, part] = mt[j // 2, j % 2, i : i + 1, :]
            a_vec[:, part] = gain[:, part] * (1.0 + mt[j // 2, j % 2, per + i : per + i + 1, :])
            g_vec[:, part] = mt[j // 2, j % 2, 2 * per + i : 2 * per + i + 1, :]
    for name in ("rt", "ct", "qw", "ow", "sink"):
        loads[name].wait()

    lane = lax.broadcasted_iota(jnp.int32, (1, LANES), 1)
    first = lane % 32 < 16

    def swapped(v):
        return jnp.where(first, pltpu.roll(v, LANES - 16, 1), pltpu.roll(v, 16, 1))

    def project(gs):
        acc = jnp.zeros((len(gs) * group, 2 * LANES), f32)
        for i in range(depth // COLS):
            part = slice(i * COLS, (i + 1) * COLS)
            a = a_vec[:, part]
            s = s_vec[:, part]
            tiles = []
            for g in gs:
                r = jnp.concatenate([inv[g]] * (COLS // LANES), axis=1)
                tiles.append((rows[g, :, part].astype(f32) * r * a + s).astype(bf16))
            acc = acc + jnp.dot(jnp.concatenate(tiles, axis=0), w[part, :], preferred_element_type=f32)
        for n, g in enumerate(gs):
            fac = rt[g : g + 1, :] + ct[...]
            vq = acc[n * group : (n + 1) * group, :LANES]
            vk = acc[n * group : (n + 1) * group, LANES:]
            q2 = vq * fac[:, :LANES] + swapped(vq) * fac[:, LANES : 2 * LANES]
            k2 = vk * fac[:, 2 * LANES : 3 * LANES] + swapped(vk) * fac[:, 3 * LANES :]
            qrot[g * group : (g + 1) * group, :] = q2.astype(bf16)
            kv[WIN + g * group : WIN + (g + 1) * group, :] = k2.astype(bf16)

    project((0, 1, n_tp - 2, n_tp - 1))

    @pl.when(z > 0)
    def _():
        send(kv.at[pl.ds(WIN, WIN)], kv.at[pl.ds(WIN + count, WIN)], h_send.at[0], h_recv.at[0], {"sp": z - 1}, False)

    @pl.when(z < n_sp - 1)
    def _():
        send(kv.at[pl.ds(count, WIN)], kv.at[pl.ds(0, WIN)], h_send.at[1], h_recv.at[1], {"sp": z + 1}, False)

    project(tuple(range(2, n_tp - 2)))

    rows2 = 2 * WIN
    qi = lax.broadcasted_iota(jnp.int32, (rows2, WIN), 0) % WIN
    ki = lax.broadcasted_iota(jnp.int32, (rows2, WIN), 1)
    head1 = lax.broadcasted_iota(jnp.int32, (rows2, 1), 0) >= WIN
    sink_col = jnp.where(head1, sink[0:1, 1:2], sink[0:1, 0:1])
    is_key = lane < HD
    contract = (((1,), (1,)), ((), ()))
    blocks = count // WIN

    def attend(b):
        qb = qrot[b * WIN : (b + 1) * WIN, :].astype(f32)
        q0 = jnp.where(is_key, qb, 0.0).astype(bf16)
        q1 = jnp.where(is_key, pltpu.roll(qb, HD, 1), 0.0).astype(bf16)
        qq = jnp.concatenate([q0, q1], axis=0)
        band = kv[b * WIN : (b + 3) * WIN, :]
        whole = ctx[...]
        s_band = lax.dot_general(qq, band, contract, preferred_element_type=f32)
        s_ctx = lax.dot_general(qq, whole, contract, preferred_element_type=f32)
        left = ki >= qi
        right = ki <= qi
        if b == 0:
            left = left & (z > 0)
        if b == blocks - 1:
            right = right & (z < n_sp - 1)
        s0 = jnp.where(left, s_band[:, :WIN], neg_large)
        s1 = s_band[:, WIN : 2 * WIN]
        s2 = jnp.where(right, s_band[:, 2 * WIN :], neg_large)
        top = jnp.maximum(jnp.maximum(s0, s1), s2)
        for i in range(whole.shape[0] // LANES):
            top = jnp.maximum(top, s_ctx[:, i * LANES : (i + 1) * LANES])
        m = jnp.maximum(jnp.max(top, axis=1, keepdims=True), sink_col)
        e0 = jnp.exp(s0 - m)
        e1 = jnp.exp(s1 - m)
        e2 = jnp.exp(s2 - m)
        ec = jnp.exp(s_ctx - m)
        tot = e0 + e1 + e2
        for i in range(whole.shape[0] // LANES):
            tot = tot + ec[:, i * LANES : (i + 1) * LANES]
        den = jnp.sum(tot, axis=1, keepdims=True) + jnp.exp(sink_col - m)
        r = 1.0 / den
        p_band = jnp.concatenate([e0, e1, e2], axis=1) * r
        o = jnp.dot(p_band.astype(bf16), band, preferred_element_type=f32) + jnp.dot(
            (ec * r).astype(bf16), whole, preferred_element_type=f32
        )
        res = jnp.where(is_key, pltpu.roll(o[:WIN], HD, 1), o[WIN:]).astype(bf16)
        att[t, b * WIN : (b + 1) * WIN, :] = res

    def att_piece(who, b):
        return att.at[who, pl.ds(b * WIN, WIN)]

    def att_send(b):
        mine = att_piece(t, b)
        send(mine, mine, t_send.at[2, b], t_recv.at[2, b], {"tp": t_o})
        send(mine, mine, t_send.at[0, b], t_recv.at[0, b], {"tp": t_r})
        send(mine, mine, t_send.at[1, b], t_recv.at[1, b], {"tp": t_l})
        send(mine, mine, tsib_send.at[0, b], tsib_recv.at[0, b], {"tp": sib})

    def att_take(b):
        for role, who in ((0, t_l), (1, t_r), (2, t_o)):
            got = att_piece(who, b)
            recv(got, t_recv.at[role, b], {"tp": who})
            send(got, got, tsib_send.at[1 + role, b], tsib_recv.at[1 + role, b], {"tp": sib})

    order = [*range(1, blocks - 1), 0, blocks - 1]
    for n, b in enumerate(order):
        if n == blocks - 2:
            @pl.when(z < n_sp - 1)
            def _():
                recv(kv.at[pl.ds(WIN + count, WIN)], h_recv.at[0], {"sp": z + 1})

            @pl.when(z > 0)
            def _():
                recv(kv.at[pl.ds(0, WIN)], h_recv.at[1], {"sp": z - 1})

        attend(b)
        att_send(b)
        if n >= 2:
            att_take(order[n - 2])
    att_take(order[-2])
    att_take(order[-1])
    for b in order:
        for role, xx in ((0, x), (1, xl), (2, xr), (3, xo)):
            recv(att_piece(xx * 2 + 1 - c, b), tsib_recv.at[role, b], {"tp": sib})

    here = pl.ds(pl.multiple_of(t * width, LANES), width)
    for n, xx in enumerate((xo, xr, xl, x)):
        part = pl.ds(pl.multiple_of(xx * WIN, WIN), WIN)
        y = jnp.zeros((WIN, width), f32)
        for i in range(n_x):
            lhs = jnp.concatenate([att[2 * i, part, :], att[2 * i + 1, part, :]], axis=1)
            y = y + jnp.dot(lhs, ow[2 * i * LANES : 2 * (i + 1) * LANES, :], preferred_element_type=f32)
        ysend[2 * n] = y[:group].astype(bf16)
        ysend[2 * n + 1] = y[group:].astype(bf16)
        if n < 3:
            for k in range(2):
                send(ysend.at[2 * n + k], yrecv.at[:, here], y_send.at[2 * n + k], y_recv.at[2 * n + c], {"tp": xx * 2 + k})
        else:
            send(ysend.at[2 * n + 1 - c], yrecv.at[:, here], y_send.at[6], y_recv.at[6], {"tp": sib})
            yrecv[:, here] = ysend[2 * n + c]
    for n, xx in enumerate((xo, xl, xr)):
        for k in range(2):
            cols = pl.ds(pl.multiple_of((xx * 2 + k) * width, LANES), width)
            recv(yrecv.at[:, cols], y_recv.at[2 * n + k], {"tp": xx * 2 + k})
    recv(yrecv.at[:, pl.ds(pl.multiple_of(sib * width, LANES), width)], y_recv.at[6], {"tp": sib})
    for i in range(depth // COLS):
        part = slice(i * COLS, (i + 1) * COLS)
        out[:, part] = (
            rows[t, :, part].astype(f32) + g_vec[:, part] * yrecv[:, part].astype(f32)
        ).astype(bf16)
    for copy in started:
        copy.wait_send()

    @pl.when(z > 0)
    def _():
        sent(kv.at[pl.ds(WIN, WIN)], h_send.at[0], {"sp": z - 1})

    @pl.when(z < n_sp - 1)
    def _():
        sent(kv.at[pl.ds(count, WIN)], h_send.at[1], {"sp": z + 1})

    @pl.when(c == 1)
    def _():
        sent(mpair.at[1], pair_send.at[0], {"tp": sib})
        sent(cown, pair_send.at[1], {"tp": sib})
        for q in range(chunks):
            for n, (g, who) in enumerate(
                ((t, t_r), (t, t_l), (sib, t_r), (sib, t_l), (t_r, t_l), (zero_l, t_r))
            ):
                sent(piece(g, q), ag_send.at[n, q], {"tp": who})
        for g in (t, t_r, t_l, zero_l, zero_r, t_o, zero_o):
            sent(rows.at[g], sib_send.at[g], {"tp": sib})
        for n, who in enumerate((t_r, t_l, t_o)):
            sent(mt.at[x], x_send.at[n], {"tp": who})
        for xx in (xr, xl, xo):
            sent(mt.at[xx], xs_send.at[xx], {"tp": sib})

    @pl.when(c == 0)
    def _():
        sent(rows.at[t], sib_send.at[t], {"tp": sib})
        sent(mt.at[x], xs_send.at[x], {"tp": sib})
        sent(cg.at[:, 1], pair_send.at[2], {"tp": sib})

        def gone(i):
            @pl.when(i != z)
            def _():
                sent(cg.at[z], c_send.at[i], {"sp": i})

            @pl.when((z == center) & (i != z))
            def _():
                sent(msum, tot_send.at[i], {"sp": i})

        each(0, n_sp, gone)

        @pl.when(z != center)
        def _():
            sent(mpair, m_send.at[0], {"sp": center})


def local(n_sp, n_tp, latent, context, conditioning, norm_gain, *rest):
    shift_w, scale_w, gate_w, q_w, k_w, v_w, o_w, sink = rest
    group, depth = latent.shape
    n_ctx = context.shape[0]
    count = n_tp * group
    width = shift_w.shape[1]
    blocks = count // WIN
    chunks = group // 16
    row_tab, col_tab = rope_tables(n_sp * count // GRID_W)
    any_space = pl.BlockSpec(memory_space=pl.ANY)
    vmem = pl.BlockSpec(memory_space=pltpu.VMEM)
    dma = pltpu.SemaphoreType.DMA
    return pl.pallas_call(
        functools.partial(kernel, n_sp, n_tp),
        out_shape=jax.ShapeDtypeStruct((group, depth), bf16),
        in_specs=[any_space] * 14,
        out_specs=vmem,
        scratch_shapes=[
            pltpu.VMEM((n_tp, group, depth), bf16),
            pltpu.VMEM((depth, 2 * LANES), bf16),
            pltpu.VMEM((2 * HD, depth), bf16),
            pltpu.VMEM(o_w.shape, bf16),
            pltpu.VMEM((3, *shift_w.shape), bf16),
            pltpu.VMEM((n_ctx, depth), bf16),
            pltpu.VMEM((n_sp, 2, n_ctx, LANES), bf16),
            pltpu.VMEM((n_ctx, LANES), bf16),
            pltpu.VMEM((2, 16, LANES), f32),
            pltpu.VMEM((n_sp, 2, 16, LANES), f32),
            pltpu.VMEM((2, 16, LANES), f32),
            pltpu.VMEM((n_tp // 2, 2, 16, LANES), f32),
            pltpu.VMEM((n_tp, group, LANES), f32),
            pltpu.VMEM((1, depth), f32),
            pltpu.VMEM((1, depth), f32),
            pltpu.VMEM((1, depth), f32),
            pltpu.VMEM((count, LANES), bf16),
            pltpu.VMEM((count + 2 * WIN, LANES), bf16),
            pltpu.VMEM((n_sp * n_ctx, LANES), bf16),
            pltpu.VMEM((n_tp, count, LANES), bf16),
            pltpu.VMEM((n_tp, group, width), bf16),
            pltpu.VMEM((group, depth), bf16),
            pltpu.VMEM((count // GRID_W, 4 * LANES), f32),
            pltpu.VMEM((GRID_W, 4 * LANES), f32),
            pltpu.VMEM((1, conditioning.shape[0]), bf16),
            pltpu.VMEM((1, depth), f32),
            pltpu.VMEM((1, sink.shape[0]), f32),
            pltpu.SemaphoreType.REGULAR,
            dma((16,)),
            dma((3,)),
            dma((3,)),
            dma((1,)),
            dma((n_sp,)),
            dma((n_sp,)),
            dma,
            dma((n_sp,)),
            dma((n_sp,)),
            dma((6, chunks)),
            dma((6, chunks)),
            dma((n_tp,)),
            dma((n_tp,)),
            dma((3,)),
            dma((n_tp // 2,)),
            dma((n_tp // 2,)),
            dma((n_tp // 2,)),
            dma((2,)),
            dma((2,)),
            dma((3, blocks)),
            dma((3, blocks)),
            dma((4, blocks)),
            dma((4, blocks)),
            dma((8,)),
            dma((8,)),
        ],
        compiler_params=pltpu.CompilerParams(
            collective_id=0, has_side_effects=True, vmem_limit_bytes=56 * 1024 * 1024
        ),
    )(
        latent,
        context,
        conditioning.reshape(1, -1),
        norm_gain.reshape(1, -1),
        shift_w,
        scale_w,
        gate_w,
        q_w,
        k_w.T,
        v_w.T,
        o_w,
        sink.reshape(1, -1),
        jnp.asarray(row_tab),
        jnp.asarray(col_tab),
    )


def solution(mesh):
    in_specs = (
        P(("grp", "sp", "tp"), None),
        P(("grp", "sp"), None),
        P(("grp", "sp")),
        P(),
        P("sp", "tp"),
        P("sp", "tp"),
        P("sp", "tp"),
        P(None, "tp"),
        P(None, "tp"),
        P(None, "tp"),
        P(None, "tp"),
        P("tp"),
    )
    return jax.shard_map(
        functools.partial(local, mesh.shape["sp"], mesh.shape["tp"]),
        mesh=mesh,
        in_specs=in_specs,
        out_specs=P(("grp", "sp", "tp"), None),
        check_vma=False,
    )
```

time: 108 us -> 118 us (1.093)
  Pallas kernels: 102 us -> 116 us
  local copies, waits for them, and re-layouts: 5.68 us -> 1.87 us
    pallas_call x1, Pallas kernels: 102 us -> 116 us  [local(): pl.pallas_call(functools.partial(kernel, n_sp, n_tp), out_shape=jax.Shape...]
    unnamed x5 -> x1, local copies, waits for them, and re-layouts: 5.68 us -> 1.87 us
where the time goes in v2:
time: 118 us
  Pallas kernels  116 us (98%)
  local copies, waits for them, and re-layouts  1.87 us (2%)
    pallas_call x1, Pallas kernels, local(): pl.pallas_call(functools.partial(kernel, n_sp, n_tp), out_shape=jax.Shape...  116 us

profile of v2, /device:TPU:33, one launch (start us, length us, event | category | flops | bytes accessed | tf_op | source)
XLA Modules:
  0.0 117.5 jit_solution(14360160774960069291)
XLA Ops:
  0.0 115.7 %shard_map.136 = bf16[64,4096]{1,0:T(8,128)(2,1)} custom-call(bf16[64,4096]{1,0:T(8,128)(2,1)} %latent.1, bf16[24,4096]{1,0:T(8,128)(2,1)} %context.1, bf16[1,128]{1,0:T(2,128)(2,1)} %bitcast.8, f32[1,4096]{1,0:T(1,128)} %bitcast.7, bf16[128,512]{1,0:T(8,128)(2,1)} %shift_w.1, bf16[128,512]{1,0:T(8,128)(2,1)} %scale_w.1, bf16[128,512]{1,0:T(8,128)(2,1)} %gate_w.1, ...), custom_call_target="tpu_custom_call" | custom-call | tf_op jit(solution)/shard_map/pallas_call | solution.py:620
  115.7 1.9 %copy.16 = bf16[64,4096]{1,0:T(8,128)(2,1)} copy(bf16[64,4096]{1,0:T(8,128)(2,1)} %shard_map.136) | data formatting | bytes 1048576

commit v3 on v2

--- a/solution.py
+++ b/solution.py
@@ -13,6 +13,7 @@
 HD = 64
 GRID_W = 64
 WIN = 128
+SPAN = 4
 LANES = 128
 COLS = 512
 
@@ -73,6 +74,7 @@
     ctx_rows,
     cg,
     cown,
+    cpair,
     mpair,
     mall,
     msum,
@@ -101,7 +103,10 @@
     tot_send,
     tot_recv,
     c_send,
-    c_recv,
+    p_recv,
+    b_recv,
+    bl_send,
+    bm_send,
     ag_send,
     ag_recv,
     sib_send,
@@ -176,13 +181,21 @@
         for who in (sib, t_r, t_l, t_o):
             greet({"tp": who})
 
-    @pl.when(c == 0)
-    def _():
-        each(z + 1, n_sp, lambda i: greet({"sp": i}))
+    lead = SPAN * (z // SPAN) + center
+    members = [(z // SPAN) * SPAN + j for j in range(SPAN) if j != center]
+    teams = n_sp // SPAN
+    team = z // SPAN
 
     @pl.when((c == 0) & (z == center))
     def _():
         each(0, center, lambda i: greet({"sp": i}))
+        each(center + 1, n_sp, lambda i: greet({"sp": i}))
+
+    @pl.when((c == 0) & (z == lead))
+    def _():
+        for i in members:
+            greet({"sp": i})
+        each(team + 1, teams, lambda i: greet({"sp": SPAN * i + center}))
 
     grid_rows = count // GRID_W
     loads = {}
@@ -208,7 +221,7 @@
     load("ow", o_w, ow)
 
     def contact():
-        pl.semaphore_wait(barrier, c * 3 + (1 - c) * (1 + z + jnp.where(z < center, 1, 0)))
+        pl.semaphore_wait(barrier, c * 3 + (1 - c) * (1 + jnp.where(z == center, 0, 1) + jnp.where(z == lead, team, 1)))
 
     def modulation():
         loads["cond"].wait()
@@ -266,7 +279,7 @@
         send(mpair.at[1], mpair.at[1], pair_send.at[0], pair_recv.at[0], {"tp": sib}, False)
 
     def hand_context():
-        send(cown, cg.at[z, 1], pair_send.at[1], pair_recv.at[1], {"tp": sib}, False)
+        send(cown, cpair.at[1], pair_send.at[1], pair_recv.at[1], {"tp": sib}, False)
 
     def sibling_rows():
         recv(rows.at[sib], sib_recv.at[sib], {"tp": sib})
@@ -350,47 +363,81 @@
             mall[center] = mpair[...]
 
         own_context()
-        cg[z, 0] = cown[...]
+        cpair[0] = cown[...]
         row_stats(t)
-        recv(cg.at[z, 1], pair_recv.at[1], {"tp": sib})
-
-        def give(i):
-            send(cg.at[z], cg.at[z], c_send.at[i], c_recv.at[z], {"sp": i}, False)
-
-        def answer(i):
-            recv(cg.at[i], c_recv.at[i], {"sp": i})
-            give(i)
-
-        each(0, z, give)
-        each(z + 1, n_sp, answer)
-
-        @pl.when(z == center)
-        def _():
+        recv(cpair.at[1], pair_recv.at[1], {"tp": sib})
+
+        def block(i):
+            return cg.at[pl.ds(SPAN * i, SPAN)]
+
+        def tell_sum():
             def take(i):
-                @pl.when(i != center)
-                def _():
-                    recv(mall.at[i], m_recv.at[i], {"sp": i})
-
-            each(0, n_sp, take)
+                recv(mall.at[i], m_recv.at[i], {"sp": i})
+
+            each(0, center, take)
+            each(center + 1, n_sp, take)
             tot = mall[0]
             for i in range(1, n_sp):
                 tot = tot + mall[i]
             msum[...] = tot
 
             def tell(i):
-                @pl.when(i != center)
-                def _():
-                    send(msum, mt.at[x], tot_send.at[i], tot_recv, {"sp": i}, False)
-
-            each(0, n_sp, tell)
+                send(msum, mt.at[x], tot_send.at[i], tot_recv, {"sp": i}, False)
+
+            each(0, center, tell)
+            each(center + 1, n_sp, tell)
             mt[x] = tot
 
-        @pl.when(z != center)
-        def _():
+        def pass_sum():
+            send(mt.at[x], mt.at[x], xs_send.at[x], xs_recv.at[x], {"tp": sib}, False)
+
+        def sum_in():
             recv(mt.at[x], tot_recv, {"sp": center})
-
-        send(mt.at[x], mt.at[x], xs_send.at[x], xs_recv.at[x], {"tp": sib}, False)
-        each(0, z, lambda i: recv(cg.at[i], c_recv.at[i], {"sp": i}))
+            pass_sum()
+
+        @pl.when(z != lead)
+        def _():
+            send(cpair, cg.at[z], c_send.at[0], p_recv.at[z % SPAN], {"sp": lead}, False)
+            sum_in()
+            each(0, teams, lambda i: recv(block(i), b_recv.at[i], {"sp": lead}))
+
+        @pl.when(z == lead)
+        def _():
+            cg[z] = cpair[...]
+
+            @pl.when(z == center)
+            def _():
+                tell_sum()
+                pass_sum()
+
+            for n, i in enumerate(members):
+                recv(cg.at[i], p_recv.at[n + (1 if n >= center else 0)], {"sp": i})
+
+            def hand_block(i):
+                for n, who in enumerate(members):
+                    send(block(i), block(i), bm_send.at[n, i], b_recv.at[i], {"sp": who}, False)
+
+            def give(i):
+                send(block(team), block(team), bl_send.at[i], b_recv.at[team], {"sp": SPAN * i + center}, False)
+
+            def got(i):
+                recv(block(i), b_recv.at[i], {"sp": SPAN * i + center})
+
+            def answer(i):
+                got(i)
+                give(i)
+                hand_block(i)
+
+            def follow(i):
+                got(i)
+                hand_block(i)
+
+            each(0, team, give)
+            hand_block(team)
+            each(team + 1, teams, answer)
+            pl.when(z != center)(sum_in)
+            each(0, team, follow)
+
         send(cg.at[:, 1], cg.at[:, 1], pair_send.at[2], pair_recv.at[2], {"tp": sib}, False)
         for g in (sib, t_r + 1, t_l + 1, t_r, t_l, t_o + 1, t_o):
             recv(rows.at[g], sib_recv.at[g], {"tp": sib})
@@ -589,16 +636,31 @@
         sent(mt.at[x], xs_send.at[x], {"tp": sib})
         sent(cg.at[:, 1], pair_send.at[2], {"tp": sib})
 
-        def gone(i):
-            @pl.when(i != z)
-            def _():
-                sent(cg.at[z], c_send.at[i], {"sp": i})
-
-            @pl.when((z == center) & (i != z))
-            def _():
-                sent(msum, tot_send.at[i], {"sp": i})
-
-        each(0, n_sp, gone)
+        def told(i):
+            sent(msum, tot_send.at[i], {"sp": i})
+
+        @pl.when(z == center)
+        def _():
+            each(0, center, told)
+            each(center + 1, n_sp, told)
+
+        @pl.when(z != lead)
+        def _():
+            sent(cpair, c_send.at[0], {"sp": lead})
+
+        @pl.when(z == lead)
+        def _():
+            def given(i):
+                sent(cg.at[pl.ds(SPAN * team, SPAN)], bl_send.at[i], {"sp": SPAN * i + center})
+
+            each(0, team, given)
+            each(team + 1, teams, given)
+
+            def handed(i):
+                for n, who in enumerate(members):
+                    sent(cg.at[pl.ds(SPAN * i, SPAN)], bm_send.at[n, i], {"sp": who})
+
+            each(0, teams, handed)
 
         @pl.when(z != center)
         def _():
@@ -631,6 +693,7 @@
             pltpu.VMEM((n_ctx, depth), bf16),
             pltpu.VMEM((n_sp, 2, n_ctx, LANES), bf16),
             pltpu.VMEM((n_ctx, LANES), bf16),
+            pltpu.VMEM((2, n_ctx, LANES), bf16),
             pltpu.VMEM((2, 16, LANES), f32),
             pltpu.VMEM((n_sp, 2, 16, LANES), f32),
             pltpu.VMEM((2, 16, LANES), f32),
@@ -658,8 +721,11 @@
             dma((n_sp,)),
             dma((n_sp,)),
             dma,
-            dma((n_sp,)),
-            dma((n_sp,)),
+            dma((1,)),
+            dma((SPAN,)),
+            dma((n_sp // SPAN,)),
+            dma((n_sp // SPAN,)),
+            dma((SPAN - 1, n_sp // SPAN)),
             dma((6, chunks)),
             dma((6, chunks)),
             dma((n_tp,)),

time: 118 us -> 95.3 us (0.81)
  Pallas kernels: 116 us -> 93.2 us
    pallas_call x1, Pallas kernels: 116 us -> 93.2 us  [local(): pl.pallas_call(functools.partial(kernel, n_sp, n_tp), out_shape=jax.Shape...]
where the time goes in v3:
time: 95.3 us; the launch traced here: 95.1 us
  Pallas kernels  93.2 us (98%)
  local copies, waits for them, and re-layouts  1.87 us (2%)
    pallas_call x1, Pallas kernels, local(): pl.pallas_call(functools.partial(kernel, n_sp, n_tp), out_shape=jax.Shape...  93.2 us

profile of v3, /device:TPU:33, one launch (start us, length us, event | category | flops | bytes accessed | tf_op | source)
XLA Modules:
  0.0 95.1 jit_solution(14727841915961743117)
XLA Ops:
  0.0 93.2 %shard_map.136 = bf16[64,4096]{1,0:T(8,128)(2,1)} custom-call(bf16[64,4096]{1,0:T(8,128)(2,1)} %latent.1, bf16[24,4096]{1,0:T(8,128)(2,1)} %context.1, bf16[1,128]{1,0:T(2,128)(2,1)} %bitcast.8, f32[1,4096]{1,0:T(1,128)} %bitcast.7, bf16[128,512]{1,0:T(8,128)(2,1)} %shift_w.1, bf16[128,512]{1,0:T(8,128)(2,1)} %scale_w.1, bf16[128,512]{1,0:T(8,128)(2,1)} %gate_w.1, ...), custom_call_target="tpu_custom_call" | custom-call | tf_op jit(solution)/shard_map/pallas_call | solution.py:682
  93.2 1.9 %copy.16 = bf16[64,4096]{1,0:T(8,128)(2,1)} copy(bf16[64,4096]{1,0:T(8,128)(2,1)} %shard_map.136) | data formatting | bytes 1048576

commit v4 on v3

--- a/solution.py
+++ b/solution.py
@@ -14,6 +14,7 @@
 GRID_W = 64
 WIN = 128
 SPAN = 4
+LATEST = 2
 LANES = 128
 COLS = 512
 
@@ -178,7 +179,7 @@
 
     @pl.when(c == 1)
     def _():
-        for who in (sib, t_r, t_l, t_o):
+        for who in (sib, t_r, t_l):
             greet({"tp": who})
 
     lead = SPAN * (z // SPAN) + center
@@ -221,7 +222,7 @@
     load("ow", o_w, ow)
 
     def contact():
-        pl.semaphore_wait(barrier, c * 3 + (1 - c) * (1 + jnp.where(z == center, 0, 1) + jnp.where(z == lead, team, 1)))
+        pl.semaphore_wait(barrier, c * 2 + (1 - c) * (1 + jnp.where(z == center, 0, 1) + jnp.where(z == lead, team, 1)))
 
     def modulation():
         loads["cond"].wait()
@@ -290,6 +291,15 @@
     def hand(groups):
         for g in groups:
             send(rows.at[g], rows.at[g], sib_send.at[g], sib_recv.at[g], {"tp": sib}, False)
+
+    def exchange():
+        for n, who in enumerate((t_r, t_l, t_o)):
+            send(mt.at[x], mt.at[x], x_send.at[n], x_recv.at[x], {"tp": who}, False)
+        for who, xx in ((t_r, xr), (t_l, xl), (t_o, xo)):
+            recv(mt.at[xx], x_recv.at[xx], {"tp": who})
+
+    def own_block(k, i):
+        return cg.at[k, pl.ds(SPAN * i, SPAN)]
 
     @pl.when(c == 1)
     def _():
@@ -337,13 +347,8 @@
             hand((t, t_r, t_l, zero_l, zero_r, t_o, zero_o))
 
         row_stats(sib)
-        recv(mt.at[x], xs_recv.at[x], {"tp": sib})
-        for n, (who, xx) in enumerate(((t_r, xr), (t_l, xl), (t_o, xo))):
-            send(mt.at[x], mt.at[x], x_send.at[n], x_recv.at[x], {"tp": who}, False)
-        for who, xx in ((t_r, xr), (t_l, xl), (t_o, xo)):
-            recv(mt.at[xx], x_recv.at[xx], {"tp": who})
-            send(mt.at[xx], mt.at[xx], xs_send.at[xx], xs_recv.at[xx], {"tp": sib}, False)
-        recv(cg.at[:, 1], pair_recv.at[2], {"tp": sib})
+        recv(mt.at[x], xs_recv, {"tp": sib})
+        exchange()
 
     @pl.when(c == 0)
     def _():
@@ -368,7 +373,7 @@
         recv(cpair.at[1], pair_recv.at[1], {"tp": sib})
 
         def block(i):
-            return cg.at[pl.ds(SPAN * i, SPAN)]
+            return cg.at[:, pl.ds(SPAN * i, SPAN)]
 
         def tell_sum():
             def take(i):
@@ -388,65 +393,63 @@
             each(center + 1, n_sp, tell)
             mt[x] = tot
 
-        def pass_sum():
-            send(mt.at[x], mt.at[x], xs_send.at[x], xs_recv.at[x], {"tp": sib}, False)
-
         def sum_in():
             recv(mt.at[x], tot_recv, {"sp": center})
-            pass_sum()
+
+        def early_rows():
+            for g in (sib, t_r + 1, t_l + 1, t_o + 1, t_r, t_l, t_o):
+                recv(rows.at[g], sib_recv.at[g], {"tp": sib})
+                row_stats(g)
 
         @pl.when(z != lead)
         def _():
-            send(cpair, cg.at[z], c_send.at[0], p_recv.at[z % SPAN], {"sp": lead}, False)
-            sum_in()
-            each(0, teams, lambda i: recv(block(i), b_recv.at[i], {"sp": lead}))
+            send(cpair, cg.at[:, z], c_send.at[0], p_recv.at[z % SPAN], {"sp": lead}, False)
+
+        def hand_block(i):
+            for n, who in enumerate(members):
+                for k in range(2):
+                    send(own_block(k, i), own_block(k, i), bm_send.at[k, n, i], b_recv.at[i], {"sp": who, "tp": t + k}, False)
+            send(own_block(1, i), own_block(1, i), bm_send.at[0, SPAN - 1, i], b_recv.at[i], {"tp": sib}, False)
+
+        def give(i):
+            send(block(team), block(team), bl_send.at[i], b_recv.at[team], {"sp": SPAN * i + center}, False)
+
+        def got(i):
+            recv(block(i), b_recv.at[i], {"sp": SPAN * i + center})
+
+        def answer(i):
+            got(i)
+            give(i)
+            hand_block(i)
+
+        def follow(i):
+            got(i)
+            hand_block(i)
+
+        tail = jnp.where(z == center, teams - LATEST, teams)
 
         @pl.when(z == lead)
         def _():
-            cg[z] = cpair[...]
-
-            @pl.when(z == center)
-            def _():
-                tell_sum()
-                pass_sum()
-
+            for k in range(2):
+                cg[k, z] = cpair[k]
             for n, i in enumerate(members):
-                recv(cg.at[i], p_recv.at[n + (1 if n >= center else 0)], {"sp": i})
-
-            def hand_block(i):
-                for n, who in enumerate(members):
-                    send(block(i), block(i), bm_send.at[n, i], b_recv.at[i], {"sp": who}, False)
-
-            def give(i):
-                send(block(team), block(team), bl_send.at[i], b_recv.at[team], {"sp": SPAN * i + center}, False)
-
-            def got(i):
-                recv(block(i), b_recv.at[i], {"sp": SPAN * i + center})
-
-            def answer(i):
-                got(i)
-                give(i)
-                hand_block(i)
-
-            def follow(i):
-                got(i)
-                hand_block(i)
-
+                recv(cg.at[:, i], p_recv.at[n + (1 if n >= center else 0)], {"sp": i})
             each(0, team, give)
             hand_block(team)
-            each(team + 1, teams, answer)
-            pl.when(z != center)(sum_in)
+            each(team + 1, tail, answer)
+
+        early_rows()
+        pl.when(z == center)(tell_sum)
+        pl.when(z != center)(sum_in)
+        send(mt.at[x], mt.at[x], xs_send, xs_recv, {"tp": sib}, False)
+
+        @pl.when(z == lead)
+        def _():
+            each(tail, teams, answer)
             each(0, team, follow)
 
-        send(cg.at[:, 1], cg.at[:, 1], pair_send.at[2], pair_recv.at[2], {"tp": sib}, False)
-        for g in (sib, t_r + 1, t_l + 1, t_r, t_l, t_o + 1, t_o):
-            recv(rows.at[g], sib_recv.at[g], {"tp": sib})
-            row_stats(g)
-        for xx in (xr, xl, xo):
-            recv(mt.at[xx], xs_recv.at[xx], {"tp": sib})
-
-    for j in range(n_sp):
-        ctx[pl.ds(j * n_ctx, n_ctx), :] = cg[j, c]
+        exchange()
+
     for j in range(n_tp):
         for i in range(per):
             part = slice(j * width + i * LANES, j * width + (i + 1) * LANES)
@@ -494,6 +497,13 @@
 
     project(tuple(range(2, n_tp - 2)))
 
+    @pl.when((c == 1) | (z != lead))
+    def _():
+        for i in range(n_sp // SPAN):
+            recv(own_block(c, i), b_recv.at[i], {"sp": lead, "tp": t - c})
+
+    for j in range(n_sp):
+        ctx[pl.ds(j * n_ctx, n_ctx), :] = cg[c, j]
     rows2 = 2 * WIN
     qi = lax.broadcasted_iota(jnp.int32, (rows2, WIN), 0) % WIN
     ki = lax.broadcasted_iota(jnp.int32, (rows2, WIN), 1)
@@ -578,6 +588,7 @@
         for role, xx in ((0, x), (1, xl), (2, xr), (3, xo)):
             recv(att_piece(xx * 2 + 1 - c, b), tsib_recv.at[role, b], {"tp": sib})
 
+    before = len(started)
     here = pl.ds(pl.multiple_of(t * width, LANES), width)
     for n, xx in enumerate((xo, xr, xl, x)):
         part = pl.ds(pl.multiple_of(xx * WIN, WIN), WIN)
@@ -593,6 +604,68 @@
         else:
             send(ysend.at[2 * n + 1 - c], yrecv.at[:, here], y_send.at[6], y_recv.at[6], {"tp": sib})
             yrecv[:, here] = ysend[2 * n + c]
+    for n, who in enumerate((t_r, t_l, t_o)):
+        sent(mt.at[x], x_send.at[n], {"tp": who})
+
+    for copy in started[:before]:
+        copy.wait_send()
+
+    @pl.when(z > 0)
+    def _():
+        sent(kv.at[pl.ds(WIN, WIN)], h_send.at[0], {"sp": z - 1})
+
+    @pl.when(z < n_sp - 1)
+    def _():
+        sent(kv.at[pl.ds(count, WIN)], h_send.at[1], {"sp": z + 1})
+
+    @pl.when(c == 1)
+    def _():
+        sent(mpair.at[1], pair_send.at[0], {"tp": sib})
+        sent(cown, pair_send.at[1], {"tp": sib})
+        for q in range(chunks):
+            for n, (g, who) in enumerate(
+                ((t, t_r), (t, t_l), (sib, t_r), (sib, t_l), (t_r, t_l), (zero_l, t_r))
+            ):
+                sent(piece(g, q), ag_send.at[n, q], {"tp": who})
+        for g in (t, t_r, t_l, zero_l, zero_r, t_o, zero_o):
+            sent(rows.at[g], sib_send.at[g], {"tp": sib})
+    @pl.when(c == 0)
+    def _():
+        sent(rows.at[t], sib_send.at[t], {"tp": sib})
+        sent(mt.at[x], xs_send, {"tp": sib})
+
+        def told(i):
+            sent(msum, tot_send.at[i], {"sp": i})
+
+        @pl.when(z == center)
+        def _():
+            each(0, center, told)
+            each(center + 1, n_sp, told)
+
+        @pl.when(z != lead)
+        def _():
+            sent(cpair, c_send.at[0], {"sp": lead})
+
+        @pl.when(z == lead)
+        def _():
+            def given(i):
+                sent(cg.at[:, pl.ds(SPAN * team, SPAN)], bl_send.at[i], {"sp": SPAN * i + center})
+
+            each(0, team, given)
+            each(team + 1, teams, given)
+
+            def handed(i):
+                for n, who in enumerate(members):
+                    for k in range(2):
+                        sent(own_block(k, i), bm_send.at[k, n, i], {"sp": who})
+                sent(own_block(1, i), bm_send.at[0, SPAN - 1, i], {"tp": sib})
+
+            each(0, teams, handed)
+
+        @pl.when(z != center)
+        def _():
+            sent(mpair, m_send.at[0], {"sp": center})
+
     for n, xx in enumerate((xo, xl, xr)):
         for k in range(2):
             cols = pl.ds(pl.multiple_of((xx * 2 + k) * width, LANES), width)
@@ -603,68 +676,8 @@
         out[:, part] = (
             rows[t, :, part].astype(f32) + g_vec[:, part] * yrecv[:, part].astype(f32)
         ).astype(bf16)
-    for copy in started:
+    for copy in started[before:]:
         copy.wait_send()
-
-    @pl.when(z > 0)
-    def _():
-        sent(kv.at[pl.ds(WIN, WIN)], h_send.at[0], {"sp": z - 1})
-
-    @pl.when(z < n_sp - 1)
-    def _():
-        sent(kv.at[pl.ds(count, WIN)], h_send.at[1], {"sp": z + 1})
-
-    @pl.when(c == 1)
-    def _():
-        sent(mpair.at[1], pair_send.at[0], {"tp": sib})
-        sent(cown, pair_send.at[1], {"tp": sib})
-        for q in range(chunks):
-            for n, (g, who) in enumerate(
-                ((t, t_r), (t, t_l), (sib, t_r), (sib, t_l), (t_r, t_l), (zero_l, t_r))
-            ):
-                sent(piece(g, q), ag_send.at[n, q], {"tp": who})
-        for g in (t, t_r, t_l, zero_l, zero_r, t_o, zero_o):
-            sent(rows.at[g], sib_send.at[g], {"tp": sib})
-        for n, who in enumerate((t_r, t_l, t_o)):
-            sent(mt.at[x], x_send.at[n], {"tp": who})
-        for xx in (xr, xl, xo):
-            sent(mt.at[xx], xs_send.at[xx], {"tp": sib})
-
-    @pl.when(c == 0)
-    def _():
-        sent(rows.at[t], sib_send.at[t], {"tp": sib})
-        sent(mt.at[x], xs_send.at[x], {"tp": sib})
-        sent(cg.at[:, 1], pair_send.at[2], {"tp": sib})
-
-        def told(i):
-            sent(msum, tot_send.at[i], {"sp": i})
-
-        @pl.when(z == center)
-        def _():
-            each(0, center, told)
-            each(center + 1, n_sp, told)
-
-        @pl.when(z != lead)
-        def _():
-            sent(cpair, c_send.at[0], {"sp": lead})
-
-        @pl.when(z == lead)
-        def _():
-            def given(i):
-                sent(cg.at[pl.ds(SPAN * team, SPAN)], bl_send.at[i], {"sp": SPAN * i + center})
-
-            each(0, team, given)
-            each(team + 1, teams, given)
-
-            def handed(i):
-                for n, who in enumerate(members):
-                    sent(cg.at[pl.ds(SPAN * i, SPAN)], bm_send.at[n, i], {"sp": who})
-
-            each(0, teams, handed)
-
-        @pl.when(z != center)
-        def _():
-            sent(mpair, m_send.at[0], {"sp": center})
 
 
 def local(n_sp, n_tp, latent, context, conditioning, norm_gain, *rest):
@@ -691,7 +704,7 @@
             pltpu.VMEM(o_w.shape, bf16),
             pltpu.VMEM((3, *shift_w.shape), bf16),
             pltpu.VMEM((n_ctx, depth), bf16),
-            pltpu.VMEM((n_sp, 2, n_ctx, LANES), bf16),
+            pltpu.VMEM((2, n_sp, n_ctx, LANES), bf16),
             pltpu.VMEM((n_ctx, LANES), bf16),
             pltpu.VMEM((2, n_ctx, LANES), bf16),
             pltpu.VMEM((2, 16, LANES), f32),
@@ -725,15 +738,15 @@
             dma((SPAN,)),
             dma((n_sp // SPAN,)),
             dma((n_sp // SPAN,)),
-            dma((SPAN - 1, n_sp // SPAN)),
+            dma((2, SPAN, n_sp // SPAN)),
             dma((6, chunks)),
             dma((6, chunks)),
             dma((n_tp,)),
             dma((n_tp,)),
             dma((3,)),
             dma((n_tp // 2,)),
-            dma((n_tp // 2,)),
-            dma((n_tp // 2,)),
+            dma,
+            dma,
             dma((2,)),
             dma((2,)),
             dma((3, blocks)),

time: 95.3 us -> 91.9 us (0.964)
  Pallas kernels: 93.2 us -> 89.9 us
    pallas_call x1, Pallas kernels: 93.2 us -> 89.9 us  [local(): pl.pallas_call(functools.partial(kernel, n_sp, n_tp), out_shape=jax.Shape...]
where the time goes in v4:
time: 91.9 us; the launch traced here: 91.8 us
  Pallas kernels  89.9 us (98%)
  local copies, waits for them, and re-layouts  1.87 us (2%)
    pallas_call x1, Pallas kernels, local(): pl.pallas_call(functools.partial(kernel, n_sp, n_tp), out_shape=jax.Shape...  89.9 us
    unnamed x1, local copies, waits for them, and re-layouts  1.87 us

profile of v4, /device:TPU:33, one launch (start us, length us, event | category | flops | bytes accessed | tf_op | source)
XLA Modules:
  0.0 91.8 jit_solution(9192268427439600913)
XLA Ops:
  0.0 89.9 %shard_map.136 = bf16[64,4096]{1,0:T(8,128)(2,1)} custom-call(bf16[64,4096]{1,0:T(8,128)(2,1)} %latent.1, bf16[24,4096]{1,0:T(8,128)(2,1)} %context.1, bf16[1,128]{1,0:T(2,128)(2,1)} %bitcast.8, f32[1,4096]{1,0:T(1,128)} %bitcast.7, bf16[128,512]{1,0:T(8,128)(2,1)} %shift_w.1, bf16[128,512]{1,0:T(8,128)(2,1)} %scale_w.1, bf16[128,512]{1,0:T(8,128)(2,1)} %gate_w.1, ...), custom_call_target="tpu_custom_call" | custom-call | tf_op jit(solution)/shard_map/pallas_call | solution.py:695
  89.9 1.9 %copy.16 = bf16[64,4096]{1,0:T(8,128)(2,1)} copy(bf16[64,4096]{1,0:T(8,128)(2,1)} %shard_map.136) | data formatting | bytes 1048576

commit v5 on v4

--- a/solution.py
+++ b/solution.py
@@ -14,7 +14,7 @@
 GRID_W = 64
 WIN = 128
 SPAN = 4
-LATEST = 2
+LATEST = 4
 LANES = 128
 COLS = 512
 
@@ -67,6 +67,7 @@
     row_tab,
     col_tab,
     out,
+    gate_out,
     rows,
     w,
     kvt,
@@ -89,7 +90,6 @@
     ctx,
     att,
     ysend,
-    yrecv,
     rt,
     ct,
     cond,
@@ -427,6 +427,7 @@
             hand_block(i)
 
         tail = jnp.where(z == center, teams - LATEST, teams)
+        pl.when(z == center)(early_rows)
 
         @pl.when(z == lead)
         def _():
@@ -438,7 +439,7 @@
             hand_block(team)
             each(team + 1, tail, answer)
 
-        early_rows()
+        pl.when(z != center)(early_rows)
         pl.when(z == center)(tell_sum)
         pl.when(z != center)(sum_in)
         send(mt.at[x], mt.at[x], xs_send, xs_recv, {"tp": sib}, False)
@@ -456,6 +457,8 @@
             s_vec[:, part] = mt[j // 2, j % 2, i : i + 1, :]
             a_vec[:, part] = gain[:, part] * (1.0 + mt[j // 2, j % 2, per + i : per + i + 1, :])
             g_vec[:, part] = mt[j // 2, j % 2, 2 * per + i : 2 * per + i + 1, :]
+    gates = pltpu.make_async_copy(g_vec, gate_out, load_sem.at[15])
+    gates.start()
     for name in ("rt", "ct", "qw", "ow", "sink"):
         loads[name].wait()
 
@@ -600,10 +603,11 @@
         ysend[2 * n + 1] = y[group:].astype(bf16)
         if n < 3:
             for k in range(2):
-                send(ysend.at[2 * n + k], yrecv.at[:, here], y_send.at[2 * n + k], y_recv.at[2 * n + c], {"tp": xx * 2 + k})
+                send(ysend.at[2 * n + k], out.at[:, here], y_send.at[2 * n + k], y_recv.at[2 * n + c], {"tp": xx * 2 + k})
         else:
-            send(ysend.at[2 * n + 1 - c], yrecv.at[:, here], y_send.at[6], y_recv.at[6], {"tp": sib})
-            yrecv[:, here] = ysend[2 * n + c]
+            send(ysend.at[2 * n + 1 - c], out.at[:, here], y_send.at[6], y_recv.at[6], {"tp": sib})
+            keep = pltpu.make_async_copy(ysend.at[2 * n + c], out.at[:, here], load_sem.at[14])
+            keep.start()
     for n, who in enumerate((t_r, t_l, t_o)):
         sent(mt.at[x], x_send.at[n], {"tp": who})
 
@@ -669,13 +673,10 @@
     for n, xx in enumerate((xo, xl, xr)):
         for k in range(2):
             cols = pl.ds(pl.multiple_of((xx * 2 + k) * width, LANES), width)
-            recv(yrecv.at[:, cols], y_recv.at[2 * n + k], {"tp": xx * 2 + k})
-    recv(yrecv.at[:, pl.ds(pl.multiple_of(sib * width, LANES), width)], y_recv.at[6], {"tp": sib})
-    for i in range(depth // COLS):
-        part = slice(i * COLS, (i + 1) * COLS)
-        out[:, part] = (
-            rows[t, :, part].astype(f32) + g_vec[:, part] * yrecv[:, part].astype(f32)
-        ).astype(bf16)
+            recv(out.at[:, cols], y_recv.at[2 * n + k], {"tp": xx * 2 + k})
+    recv(out.at[:, pl.ds(pl.multiple_of(sib * width, LANES), width)], y_recv.at[6], {"tp": sib})
+    keep.wait()
+    gates.wait()
     for copy in started[before:]:
         copy.wait_send()
 
@@ -690,13 +691,12 @@
     chunks = group // 16
     row_tab, col_tab = rope_tables(n_sp * count // GRID_W)
     any_space = pl.BlockSpec(memory_space=pl.ANY)
-    vmem = pl.BlockSpec(memory_space=pltpu.VMEM)
     dma = pltpu.SemaphoreType.DMA
-    return pl.pallas_call(
+    blended, gate = pl.pallas_call(
         functools.partial(kernel, n_sp, n_tp),
-        out_shape=jax.ShapeDtypeStruct((group, depth), bf16),
+        out_shape=(jax.ShapeDtypeStruct((group, depth), bf16), jax.ShapeDtypeStruct((1, depth), f32)),
         in_specs=[any_space] * 14,
-        out_specs=vmem,
+        out_specs=(any_space, any_space),
         scratch_shapes=[
             pltpu.VMEM((n_tp, group, depth), bf16),
             pltpu.VMEM((depth, 2 * LANES), bf16),
@@ -720,7 +720,6 @@
             pltpu.VMEM((n_sp * n_ctx, LANES), bf16),
             pltpu.VMEM((n_tp, count, LANES), bf16),
             pltpu.VMEM((n_tp, group, width), bf16),
-            pltpu.VMEM((group, depth), bf16),
             pltpu.VMEM((count // GRID_W, 4 * LANES), f32),
             pltpu.VMEM((GRID_W, 4 * LANES), f32),
             pltpu.VMEM((1, conditioning.shape[0]), bf16),
@@ -775,6 +774,7 @@
         jnp.asarray(row_tab),
         jnp.asarray(col_tab),
     )
+    return (latent.astype(f32) + gate * blended.astype(f32)).astype(bf16)
 
 
 def solution(mesh):

time: 91.9 us -> 88.6 us (0.964)
  Pallas kernels: 89.9 us -> 86.5 us
  other arithmetic: 0 us -> 1.99 us
  local copies, waits for them, and re-layouts: 1.87 us -> 0.01 us
    pallas_call x1, Pallas kernels: 89.9 us -> 86.5 us  [local(): pl.pallas_call(functools.partial(kernel, n_sp, n_tp), out_shape=(jax.Shap...]
    convert_element_type x0 -> x1, other arithmetic: none -> 1.99 us  [local(): return (latent.astype(f32) + gate * blended.astype(f32)).astype(bf16)]
    unnamed x1 -> x2, local copies, waits for them, and re-layouts: 1.87 us -> 0.01 us
where the time goes in v5:
time: 88.6 us; the launch traced here: 88.5 us
  Pallas kernels  86.5 us (98%)
  other arithmetic  1.99 us (2%)
    pallas_call x1, Pallas kernels, local(): pl.pallas_call(functools.partial(kernel, n_sp, n_tp), out_shape=(jax.Shap...  86.5 us
    convert_element_type x1, other arithmetic, local(): return (latent.astype(f32) + gate * blended.astype(f32)).astype(bf16)  1.99 us

profile of v5, /device:TPU:33, one launch (start us, length us, event | category | flops | bytes accessed | tf_op | source)
XLA Modules:
  0.0 88.5 jit_solution(18071856128478864194)
XLA Ops:
  0.0 0.0 copy-start
  0.0 86.5 %shard_map.136 = (bf16[64,4096]{1,0:T(8,128)(2,1)}, f32[1,4096]{1,0:T(1,128)}) custom-call(bf16[64,4096]{1,0:T(8,128)(2,1)} %latent.1, bf16[24,4096]{1,0:T(8,128)(2,1)} %context.1, bf16[1,128]{1,0:T(2,128)(2,1)} %bitcast.10, f32[1,4096]{1,0:T(1,128)} %bitcast.8, bf16[128,512]{1,0:T(8,128)(2,1)} %shift_w.1, bf16[128,512]{1,0:T(8,128)(2,1)} %scale_w.1, ...), custom_call_target="tpu_custom_call" | custom-call | tf_op jit(solution)/shard_map/pallas_call | solution.py:695
  86.5 0.0 copy-done
  86.5 2.0 %add_convert_fusion = bf16[64,4096]{1,0:T(8,128)(2,1)} fusion(bf16[64,4096]{1,0:T(8,128)(2,1)} %get-tuple-element.8, bf16[64,4096]{1,0:T(8,128)(2,1)S(1)} %copy-done, f32[4096]{0:T(1024)} %bitcast.9), kind=kLoop, calls=%fused_computation | loop fusion | flops 1310720 | bytes 1589248 | tf_op jit(solution)/shard_map/convert_element_type | solution.py:777
Async XLA Ops:
  0.0 86.5 %copy-start = (bf16[64,4096]{1,0:T(8,128)(2,1)S(1)}, bf16[64,4096]{1,0:T(8,128)(2,1)}, u32[]{:S(2)}) copy-start(bf16[64,4096]{1,0:T(8,128)(2,1)} %latent.1) | copy-start | bytes 1572868

commit v6 on v5

--- a/solution.py
+++ b/solution.py
@@ -114,8 +114,6 @@
     sib_recv,
     x_send,
     x_recv,
-    xs_send,
-    xs_recv,
     h_send,
     h_recv,
     t_send,
@@ -179,7 +177,7 @@
 
     @pl.when(c == 1)
     def _():
-        for who in (sib, t_r, t_l):
+        for who in (sib, t_l):
             greet({"tp": who})
 
     lead = SPAN * (z // SPAN) + center
@@ -222,7 +220,7 @@
     load("ow", o_w, ow)
 
     def contact():
-        pl.semaphore_wait(barrier, c * 2 + (1 - c) * (1 + jnp.where(z == center, 0, 1) + jnp.where(z == lead, team, 1)))
+        pl.semaphore_wait(barrier, 1 + jnp.where(z == center, 0, 1) + jnp.where(z == lead, team, 1))
 
     def modulation():
         loads["cond"].wait()
@@ -285,38 +283,35 @@
     def sibling_rows():
         recv(rows.at[sib], sib_recv.at[sib], {"tp": sib})
         for q in range(chunks):
-            send(piece(sib, q), piece(sib, q), ag_send.at[2, q], ag_recv.at[2, q], {"tp": t_r}, False)
-            send(piece(sib, q), piece(sib, q), ag_send.at[3, q], ag_recv.at[3, q], {"tp": t_l}, False)
+            send(piece(sib, q), piece(sib, q), ag_send.at[2], ag_recv.at[2, q], {"tp": t_r}, False)
+            send(piece(sib, q), piece(sib, q), ag_send.at[3], ag_recv.at[3, q], {"tp": t_l}, False)
 
     def hand(groups):
         for g in groups:
             send(rows.at[g], rows.at[g], sib_send.at[g], sib_recv.at[g], {"tp": sib}, False)
 
-    def exchange():
-        for n, who in enumerate((t_r, t_l, t_o)):
-            send(mt.at[x], mt.at[x], x_send.at[n], x_recv.at[x], {"tp": who}, False)
-        for who, xx in ((t_r, xr), (t_l, xl), (t_o, xo)):
-            recv(mt.at[xx], x_recv.at[xx], {"tp": who})
-
     def own_block(k, i):
         return cg.at[k, pl.ds(SPAN * i, SPAN)]
 
     @pl.when(c == 1)
     def _():
+        modulation()
         loads["rows"].wait()
-        contact()
+        pl.semaphore_wait(barrier, 1)
+        pl.when(~late & (z >= n_sp // 2))(meet)
         for q in range(chunks):
-            send(piece(t, q), piece(t, q), ag_send.at[0, q], ag_recv.at[0, q], {"tp": t_r}, False)
-            send(piece(t, q), piece(t, q), ag_send.at[1, q], ag_recv.at[1, q], {"tp": t_l}, False)
-        modulation()
-        pl.when(~late)(meet)
+            send(piece(t, q), piece(t, q), ag_send.at[0], ag_recv.at[0, q], {"tp": t_r}, False)
         own_context()
+        recv(piece(t_l, 0), ag_recv.at[0, 0], {"tp": t_l})
+        for q in range(chunks):
+            send(piece(t, q), piece(t, q), ag_send.at[1], ag_recv.at[1, q], {"tp": t_l}, False)
+        pl.when(~late & (z < n_sp // 2))(meet)
         pl.when(~late)(hand_context)
         pl.when(~late)(sibling_rows)
         for q in range(chunks):
             recv(piece(t_r, q), ag_recv.at[1, q], {"tp": t_r})
-            send(piece(t_r, q), piece(t_r, q), ag_send.at[4, q], ag_recv.at[4, q], {"tp": t_l}, False)
-        for q in range(chunks):
+            send(piece(t_r, q), piece(t_r, q), ag_send.at[4], ag_recv.at[4, q], {"tp": t_l}, False)
+        for q in range(1, chunks):
             recv(piece(t_l, q), ag_recv.at[0, q], {"tp": t_l})
         pl.when(~late)(functools.partial(hand, (t, t_r, t_l)))
         row_stats(t)
@@ -324,7 +319,7 @@
         row_stats(t_r)
         for q in range(chunks):
             recv(piece(zero_l, q), ag_recv.at[2, q], {"tp": t_l})
-            send(piece(zero_l, q), piece(zero_l, q), ag_send.at[5, q], ag_recv.at[5, q], {"tp": t_r}, False)
+            send(piece(zero_l, q), piece(zero_l, q), ag_send.at[5], ag_recv.at[5, q], {"tp": t_r}, False)
         for q in range(chunks):
             recv(piece(zero_r, q), ag_recv.at[3, q], {"tp": t_r})
         pl.when(~late)(functools.partial(hand, (zero_l, zero_r)))
@@ -347,8 +342,10 @@
             hand((t, t_r, t_l, zero_l, zero_r, t_o, zero_o))
 
         row_stats(sib)
-        recv(mt.at[x], xs_recv, {"tp": sib})
-        exchange()
+        recv(mt.at[x], x_recv.at[x], {"tp": sib})
+        for n, (xx, who) in enumerate(((xr, zero_r), (xl, zero_l), (xo, zero_o))):
+            recv(mt.at[xx], x_recv.at[xx], {"tp": who})
+            send(mt.at[xx], mt.at[xx], x_send.at[n], x_recv.at[xx], {"tp": sib}, False)
 
     @pl.when(c == 0)
     def _():
@@ -361,11 +358,7 @@
 
         @pl.when(z != center)
         def _():
-            send(mpair, mall.at[z], m_send.at[0], m_recv.at[z], {"sp": center}, False)
-
-        @pl.when(z == center)
-        def _():
-            mall[center] = mpair[...]
+            send(mpair, mall.at[z - jnp.where(z > center, 1, 0)], m_send.at[0], m_recv, {"sp": center}, False)
 
         own_context()
         cpair[0] = cown[...]
@@ -376,18 +369,14 @@
             return cg.at[:, pl.ds(SPAN * i, SPAN)]
 
         def tell_sum():
-            def take(i):
-                recv(mall.at[i], m_recv.at[i], {"sp": i})
-
-            each(0, center, take)
-            each(center + 1, n_sp, take)
-            tot = mall[0]
-            for i in range(1, n_sp):
+            recv(mall, m_recv, {"sp": 0})
+            tot = mpair[...]
+            for i in range(n_sp - 1):
                 tot = tot + mall[i]
             msum[...] = tot
 
             def tell(i):
-                send(msum, mt.at[x], tot_send.at[i], tot_recv, {"sp": i}, False)
+                send(msum, mt.at[x], tot_send, tot_recv, {"sp": i}, False)
 
             each(0, center, tell)
             each(center + 1, n_sp, tell)
@@ -396,10 +385,13 @@
         def sum_in():
             recv(mt.at[x], tot_recv, {"sp": center})
 
-        def early_rows():
-            for g in (sib, t_r + 1, t_l + 1, t_o + 1, t_r, t_l, t_o):
+        def rows_in(groups):
+            for g in groups:
                 recv(rows.at[g], sib_recv.at[g], {"tp": sib})
                 row_stats(g)
+
+        def early_rows():
+            rows_in((sib, t_r + 1, t_l + 1))
 
         @pl.when(z != lead)
         def _():
@@ -408,8 +400,8 @@
         def hand_block(i):
             for n, who in enumerate(members):
                 for k in range(2):
-                    send(own_block(k, i), own_block(k, i), bm_send.at[k, n, i], b_recv.at[i], {"sp": who, "tp": t + k}, False)
-            send(own_block(1, i), own_block(1, i), bm_send.at[0, SPAN - 1, i], b_recv.at[i], {"tp": sib}, False)
+                    send(own_block(k, i), own_block(k, i), bm_send.at[2 * n + k], b_recv.at[i], {"sp": who, "tp": t + k}, False)
+            send(own_block(1, i), own_block(1, i), bm_send.at[2 * SPAN - 2], b_recv.at[i], {"tp": sib}, False)
 
         def give(i):
             send(block(team), block(team), bl_send.at[i], b_recv.at[team], {"sp": SPAN * i + center}, False)
@@ -442,14 +434,17 @@
         pl.when(z != center)(early_rows)
         pl.when(z == center)(tell_sum)
         pl.when(z != center)(sum_in)
-        send(mt.at[x], mt.at[x], xs_send, xs_recv, {"tp": sib}, False)
+        for n, who in enumerate((sib, t_o + 1, t_r + 1, t_l + 1)):
+            send(mt.at[x], mt.at[x], x_send.at[n], x_recv.at[x], {"tp": who}, False)
 
         @pl.when(z == lead)
         def _():
             each(tail, teams, answer)
             each(0, team, follow)
 
-        exchange()
+        rows_in((t_o + 1, t_r, t_l, t_o))
+        for xx in (xr, xl, xo):
+            recv(mt.at[xx], x_recv.at[xx], {"tp": sib})
 
     for j in range(n_tp):
         for i in range(per):
@@ -559,16 +554,16 @@
 
     def att_send(b):
         mine = att_piece(t, b)
-        send(mine, mine, t_send.at[2, b], t_recv.at[2, b], {"tp": t_o})
-        send(mine, mine, t_send.at[0, b], t_recv.at[0, b], {"tp": t_r})
-        send(mine, mine, t_send.at[1, b], t_recv.at[1, b], {"tp": t_l})
-        send(mine, mine, tsib_send.at[0, b], tsib_recv.at[0, b], {"tp": sib})
+        send(mine, mine, t_send.at[2], t_recv.at[2, b], {"tp": t_o}, False)
+        send(mine, mine, t_send.at[0], t_recv.at[0, b], {"tp": t_r}, False)
+        send(mine, mine, t_send.at[1], t_recv.at[1, b], {"tp": t_l}, False)
+        send(mine, mine, tsib_send.at[0], tsib_recv.at[0], {"tp": sib}, False)
 
     def att_take(b):
         for role, who in ((0, t_l), (1, t_r), (2, t_o)):
             got = att_piece(who, b)
             recv(got, t_recv.at[role, b], {"tp": who})
-            send(got, got, tsib_send.at[1 + role, b], tsib_recv.at[1 + role, b], {"tp": sib})
+            send(got, got, tsib_send.at[1 + role], tsib_recv.at[1 + role], {"tp": sib}, False)
 
     order = [*range(1, blocks - 1), 0, blocks - 1]
     for n, b in enumerate(order):
@@ -587,9 +582,8 @@
             att_take(order[n - 2])
     att_take(order[-2])
     att_take(order[-1])
-    for b in order:
-        for role, xx in ((0, x), (1, xl), (2, xr), (3, xo)):
-            recv(att_piece(xx * 2 + 1 - c, b), tsib_recv.at[role, b], {"tp": sib})
+    for role, xx in ((0, x), (1, xl), (2, xr), (3, xo)):
+        recv(att.at[xx * 2 + 1 - c], tsib_recv.at[role], {"tp": sib})
 
     before = len(started)
     here = pl.ds(pl.multiple_of(t * width, LANES), width)
@@ -609,8 +603,9 @@
             keep = pltpu.make_async_copy(ysend.at[2 * n + c], out.at[:, here], load_sem.at[14])
             keep.start()
     for n, who in enumerate((t_r, t_l, t_o)):
-        sent(mt.at[x], x_send.at[n], {"tp": who})
-
+        sent(att.at[t], t_send.at[n], {"tp": who})
+    for n, who in enumerate((t, t_l, t_r, t_o)):
+        sent(att.at[who], tsib_send.at[n], {"tp": sib})
     for copy in started[:before]:
         copy.wait_send()
 
@@ -624,27 +619,23 @@
 
     @pl.when(c == 1)
     def _():
+        for n, xx in enumerate((xr, xl, xo)):
+            sent(mt.at[xx], x_send.at[n], {"tp": sib})
         sent(mpair.at[1], pair_send.at[0], {"tp": sib})
         sent(cown, pair_send.at[1], {"tp": sib})
-        for q in range(chunks):
-            for n, (g, who) in enumerate(
-                ((t, t_r), (t, t_l), (sib, t_r), (sib, t_l), (t_r, t_l), (zero_l, t_r))
-            ):
-                sent(piece(g, q), ag_send.at[n, q], {"tp": who})
+        for n, (g, who) in enumerate(((t, t_r), (t, t_l), (sib, t_r), (sib, t_l), (t_r, t_l), (zero_l, t_r))):
+            sent(rows.at[g], ag_send.at[n], {"tp": who})
         for g in (t, t_r, t_l, zero_l, zero_r, t_o, zero_o):
             sent(rows.at[g], sib_send.at[g], {"tp": sib})
     @pl.when(c == 0)
     def _():
         sent(rows.at[t], sib_send.at[t], {"tp": sib})
-        sent(mt.at[x], xs_send, {"tp": sib})
-
-        def told(i):
-            sent(msum, tot_send.at[i], {"sp": i})
+        for n, who in enumerate((sib, t_o + 1, t_r + 1, t_l + 1)):
+            sent(mt.at[x], x_send.at[n], {"tp": who})
 
         @pl.when(z == center)
         def _():
-            each(0, center, told)
-            each(center + 1, n_sp, told)
+            sent(mall, tot_send, {"sp": 0})
 
         @pl.when(z != lead)
         def _():
@@ -658,13 +649,10 @@
             each(0, team, given)
             each(team + 1, teams, given)
 
-            def handed(i):
-                for n, who in enumerate(members):
-                    for k in range(2):
-                        sent(own_block(k, i), bm_send.at[k, n, i], {"sp": who})
-                sent(own_block(1, i), bm_send.at[0, SPAN - 1, i], {"tp": sib})
-
-            each(0, teams, handed)
+            for n, who in enumerate(members):
+                for k in range(2):
+                    sent(cg.at[k], bm_send.at[2 * n + k], {"sp": who})
+            sent(cg.at[1], bm_send.at[2 * SPAN - 2], {"tp": sib})
 
         @pl.when(z != center)
         def _():
@@ -708,7 +696,7 @@
             pltpu.VMEM((n_ctx, LANES), bf16),
             pltpu.VMEM((2, n_ctx, LANES), bf16),
             pltpu.VMEM((2, 16, LANES), f32),
-            pltpu.VMEM((n_sp, 2, 16, LANES), f32),
+            pltpu.VMEM((n_sp - 1, 2, 16, LANES), f32),
             pltpu.VMEM((2, 16, LANES), f32),
             pltpu.VMEM((n_tp // 2, 2, 16, LANES), f32),
             pltpu.VMEM((n_tp, group, LANES), f32),
@@ -730,28 +718,26 @@
             dma((3,)),
             dma((3,)),
             dma((1,)),
-            dma((n_sp,)),
-            dma((n_sp,)),
+            dma,
+            dma,
             dma,
             dma((1,)),
             dma((SPAN,)),
             dma((n_sp // SPAN,)),
             dma((n_sp // SPAN,)),
-            dma((2, SPAN, n_sp // SPAN)),
-            dma((6, chunks)),
+            dma((2 * SPAN,)),
+            dma((6,)),
             dma((6, chunks)),
             dma((n_tp,)),
             dma((n_tp,)),
-            dma((3,)),
+            dma((4,)),
             dma((n_tp // 2,)),
-            dma,
-            dma,
             dma((2,)),
             dma((2,)),
+            dma((3,)),
             dma((3, blocks)),
-            dma((3, blocks)),
-            dma((4, blocks)),
-            dma((4, blocks)),
+            dma((4,)),
+            dma((4,)),
             dma((8,)),
             dma((8,)),
         ],

time: 88.6 us -> 87.4 us (0.986)
  Pallas kernels: 86.5 us -> 85.2 us
    pallas_call x1, Pallas kernels: 86.5 us -> 85.2 us  [local(): pl.pallas_call(functools.partial(kernel, n_sp, n_tp), out_shape=(jax.Shap...]
where the time goes in v6:
time: 87.4 us; the launch traced here: 87.2 us
  Pallas kernels  85.2 us (97%)
  other arithmetic  1.99 us (2%)
    pallas_call x1, Pallas kernels, local(): pl.pallas_call(functools.partial(kernel, n_sp, n_tp), out_shape=(jax.Shap...  85.2 us
    convert_element_type x1, other arithmetic, local(): return (latent.astype(f32) + gate * blended.astype(f32)).astype(bf16)  1.99 us

profile of v6, /device:TPU:33, one launch (start us, length us, event | category | flops | bytes accessed | tf_op | source)
XLA Modules:
  0.0 87.2 jit_solution(16096836719547709982)
XLA Ops:
  0.0 0.0 copy-start
  0.0 85.2 %shard_map.136 = (bf16[64,4096]{1,0:T(8,128)(2,1)}, f32[1,4096]{1,0:T(1,128)}) custom-call(bf16[64,4096]{1,0:T(8,128)(2,1)} %latent.1, bf16[24,4096]{1,0:T(8,128)(2,1)} %context.1, bf16[1,128]{1,0:T(2,128)(2,1)} %bitcast.10, f32[1,4096]{1,0:T(1,128)} %bitcast.8, bf16[128,512]{1,0:T(8,128)(2,1)} %shift_w.1, bf16[128,512]{1,0:T(8,128)(2,1)} %scale_w.1, ...), custom_call_target="tpu_custom_call" | custom-call | tf_op jit(solution)/shard_map/pallas_call | solution.py:683
  85.2 0.0 copy-done
  85.2 2.0 %add_convert_fusion = bf16[64,4096]{1,0:T(8,128)(2,1)} fusion(bf16[64,4096]{1,0:T(8,128)(2,1)} %get-tuple-element.8, bf16[64,4096]{1,0:T(8,128)(2,1)S(1)} %copy-done, f32[4096]{0:T(1024)} %bitcast.9), kind=kLoop, calls=%fused_computation | loop fusion | flops 1310720 | bytes 1589248 | tf_op jit(solution)/shard_map/convert_element_type | solution.py:763
Async XLA Ops:
  0.0 85.2 %copy-start = (bf16[64,4096]{1,0:T(8,128)(2,1)S(1)}, bf16[64,4096]{1,0:T(8,128)(2,1)}, u32[]{:S(2)}) copy-start(bf16[64,4096]{1,0:T(8,128)(2,1)} %latent.1) | copy-start | bytes 1572868

commit v7 on v6

--- a/solution.py
+++ b/solution.py
@@ -180,10 +180,12 @@
         for who in (sib, t_l):
             greet({"tp": who})
 
-    lead = SPAN * (z // SPAN) + center
-    members = [(z // SPAN) * SPAN + j for j in range(SPAN) if j != center]
+    slot = (z + 1) % n_sp
     teams = n_sp // SPAN
-    team = z // SPAN
+    team = slot // SPAN
+    lead = SPAN * team + center
+    members = [(z + n_sp - 1) % n_sp, (z + 1) % n_sp, (z + n_sp - 2) % n_sp]
+    places = (1, 3, 0)
 
     @pl.when((c == 0) & (z == center))
     def _():
@@ -302,11 +304,12 @@
         for q in range(chunks):
             send(piece(t, q), piece(t, q), ag_send.at[0], ag_recv.at[0, q], {"tp": t_r}, False)
         own_context()
+        pl.when(~late & (z >= n_sp // 2))(hand_context)
         recv(piece(t_l, 0), ag_recv.at[0, 0], {"tp": t_l})
         for q in range(chunks):
             send(piece(t, q), piece(t, q), ag_send.at[1], ag_recv.at[1, q], {"tp": t_l}, False)
         pl.when(~late & (z < n_sp // 2))(meet)
-        pl.when(~late)(hand_context)
+        pl.when(~late & (z < n_sp // 2))(hand_context)
         pl.when(~late)(sibling_rows)
         for q in range(chunks):
             recv(piece(t_r, q), ag_recv.at[1, q], {"tp": t_r})
@@ -395,13 +398,24 @@
 
         @pl.when(z != lead)
         def _():
-            send(cpair, cg.at[:, z], c_send.at[0], p_recv.at[z % SPAN], {"sp": lead}, False)
-
-        def hand_block(i):
-            for n, who in enumerate(members):
+            send(cpair, cg.at[:, slot], c_send.at[0], p_recv.at[slot % SPAN], {"sp": lead}, False)
+
+        def hand_near(i):
+            for n, who in enumerate(members[:2]):
                 for k in range(2):
                     send(own_block(k, i), own_block(k, i), bm_send.at[2 * n + k], b_recv.at[i], {"sp": who, "tp": t + k}, False)
             send(own_block(1, i), own_block(1, i), bm_send.at[2 * SPAN - 2], b_recv.at[i], {"tp": sib}, False)
+
+        def hand_far(i):
+            for k in range(2):
+                send(own_block(k, i), own_block(k, i), bm_send.at[4 + k], b_recv.at[i], {"sp": members[2], "tp": t + k}, False)
+
+        def hand_block(i):
+            hand_near(i)
+            hand_far(i)
+
+        def member_in(n):
+            recv(cg.at[:, SPAN * team + places[n]], p_recv.at[places[n]], {"sp": members[n]})
 
         def give(i):
             send(block(team), block(team), bl_send.at[i], b_recv.at[team], {"sp": SPAN * i + center}, False)
@@ -418,18 +432,35 @@
             got(i)
             hand_block(i)
 
-        tail = jnp.where(z == center, teams - LATEST, teams)
-        pl.when(z == center)(early_rows)
+        def near_in(i):
+            got(i)
+            hand_near(i)
+
+        def late_in(i):
+            got(i)
+            give(i)
+            hand_near(i)
 
         @pl.when(z == lead)
         def _():
             for k in range(2):
-                cg[k, z] = cpair[k]
-            for n, i in enumerate(members):
-                recv(cg.at[:, i], p_recv.at[n + (1 if n >= center else 0)], {"sp": i})
+                cg[k, slot] = cpair[k]
+            member_in(1)
+            member_in(0)
+
+        @pl.when(z == center)
+        def _():
+            early_rows()
+            each(1, teams - LATEST, near_in)
+            member_in(2)
+            hand_near(0)
+
+        @pl.when((z == lead) & (z != center))
+        def _():
+            member_in(2)
             each(0, team, give)
             hand_block(team)
-            each(team + 1, tail, answer)
+            each(team + 1, teams, answer)
 
         pl.when(z != center)(early_rows)
         pl.when(z == center)(tell_sum)
@@ -437,9 +468,14 @@
         for n, who in enumerate((sib, t_o + 1, t_r + 1, t_l + 1)):
             send(mt.at[x], mt.at[x], x_send.at[n], x_recv.at[x], {"tp": who}, False)
 
-        @pl.when(z == lead)
-        def _():
-            each(tail, teams, answer)
+        @pl.when(z == center)
+        def _():
+            each(teams - LATEST, teams, late_in)
+            each(1, teams - LATEST, give)
+            each(0, teams, hand_far)
+
+        @pl.when((z == lead) & (z != center))
+        def _():
             each(0, team, follow)
 
         rows_in((t_o + 1, t_r, t_l, t_o))

time: 87.4 us -> 88 us (level)
  no operation moved by 1% of the time
where the time goes in v7:
time: 88 us; the launch traced here: 87.8 us
  Pallas kernels  85.8 us (98%)
  other arithmetic  1.99 us (2%)
    pallas_call x1, Pallas kernels, local(): pl.pallas_call(functools.partial(kernel, n_sp, n_tp), out_shape=(jax.Shap...  85.8 us
    convert_element_type x1, other arithmetic, local(): return (latent.astype(f32) + gate * blended.astype(f32)).astype(bf16)  1.99 us

profile of v7, /device:TPU:33, one launch (start us, length us, event | category | flops | bytes accessed | tf_op | source)
XLA Modules:
  0.0 87.8 jit_solution(11151221548957133172)
XLA Ops:
  0.0 0.0 copy-start
  0.0 85.8 %shard_map.136 = (bf16[64,4096]{1,0:T(8,128)(2,1)}, f32[1,4096]{1,0:T(1,128)}) custom-call(bf16[64,4096]{1,0:T(8,128)(2,1)} %latent.1, bf16[24,4096]{1,0:T(8,128)(2,1)} %context.1, bf16[1,128]{1,0:T(2,128)(2,1)} %bitcast.10, f32[1,4096]{1,0:T(1,128)} %bitcast.8, bf16[128,512]{1,0:T(8,128)(2,1)} %shift_w.1, bf16[128,512]{1,0:T(8,128)(2,1)} %scale_w.1, ...), custom_call_target="tpu_custom_call" | custom-call | tf_op jit(solution)/shard_map/pallas_call | solution.py:719
  85.8 0.0 copy-done
  85.8 2.0 %add_convert_fusion = bf16[64,4096]{1,0:T(8,128)(2,1)} fusion(bf16[64,4096]{1,0:T(8,128)(2,1)} %get-tuple-element.8, bf16[64,4096]{1,0:T(8,128)(2,1)S(1)} %copy-done, f32[4096]{0:T(1024)} %bitcast.9), kind=kLoop, calls=%fused_computation | loop fusion | flops 1310720 | bytes 1589248 | tf_op jit(solution)/shard_map/convert_element_type | solution.py:799
Async XLA Ops:
  0.0 85.8 %copy-start = (bf16[64,4096]{1,0:T(8,128)(2,1)S(1)}, bf16[64,4096]{1,0:T(8,128)(2,1)}, u32[]{:S(2)}) copy-start(bf16[64,4096]{1,0:T(8,128)(2,1)} %latent.1) | copy-start | bytes 1572868

commit v8 on v7

--- a/solution.py
+++ b/solution.py
@@ -295,6 +295,16 @@
     def own_block(k, i):
         return cg.at[k, pl.ds(SPAN * i, SPAN)]
 
+    def block(i):
+        return cg.at[:, pl.ds(SPAN * i, SPAN)]
+
+    def hand_far(i):
+        for k in range(2):
+            send(own_block(k, i), own_block(k, i), bm_send.at[4 + k], b_recv.at[i], {"sp": members[2], "tp": t + k}, False)
+
+    def give(i):
+        send(block(team), block(team), bl_send.at[i], b_recv.at[team], {"sp": SPAN * i + center}, False)
+
     @pl.when(c == 1)
     def _():
         modulation()
@@ -368,9 +378,6 @@
         row_stats(t)
         recv(cpair.at[1], pair_recv.at[1], {"tp": sib})
 
-        def block(i):
-            return cg.at[:, pl.ds(SPAN * i, SPAN)]
-
         def tell_sum():
             recv(mall, m_recv, {"sp": 0})
             tot = mpair[...]
@@ -406,19 +413,12 @@
                     send(own_block(k, i), own_block(k, i), bm_send.at[2 * n + k], b_recv.at[i], {"sp": who, "tp": t + k}, False)
             send(own_block(1, i), own_block(1, i), bm_send.at[2 * SPAN - 2], b_recv.at[i], {"tp": sib}, False)
 
-        def hand_far(i):
-            for k in range(2):
-                send(own_block(k, i), own_block(k, i), bm_send.at[4 + k], b_recv.at[i], {"sp": members[2], "tp": t + k}, False)
-
         def hand_block(i):
             hand_near(i)
             hand_far(i)
 
         def member_in(n):
             recv(cg.at[:, SPAN * team + places[n]], p_recv.at[places[n]], {"sp": members[n]})
-
-        def give(i):
-            send(block(team), block(team), bl_send.at[i], b_recv.at[team], {"sp": SPAN * i + center}, False)
 
         def got(i):
             recv(block(i), b_recv.at[i], {"sp": SPAN * i + center})
@@ -436,11 +436,6 @@
             got(i)
             hand_near(i)
 
-        def late_in(i):
-            got(i)
-            give(i)
-            hand_near(i)
-
         @pl.when(z == lead)
         def _():
             for k in range(2):
@@ -452,9 +447,6 @@
         def _():
             early_rows()
             each(1, teams - LATEST, near_in)
-            member_in(2)
-            hand_near(0)
-
         @pl.when((z == lead) & (z != center))
         def _():
             member_in(2)
@@ -470,9 +462,10 @@
 
         @pl.when(z == center)
         def _():
-            each(teams - LATEST, teams, late_in)
+            member_in(2)
+            hand_near(0)
             each(1, teams - LATEST, give)
-            each(0, teams, hand_far)
+            each(teams - LATEST, teams, near_in)
 
         @pl.when((z == lead) & (z != center))
         def _():
@@ -528,6 +521,11 @@
     @pl.when(z < n_sp - 1)
     def _():
         send(kv.at[pl.ds(count, WIN)], kv.at[pl.ds(0, WIN)], h_send.at[1], h_recv.at[1], {"sp": z + 1}, False)
+
+    @pl.when((c == 0) & (z == center))
+    def _():
+        each(teams - LATEST, teams, give)
+        each(0, teams, hand_far)
 
     project(tuple(range(2, n_tp - 2)))
 

time: 88 us -> 85.8 us (0.975)
  Pallas kernels: 85.8 us -> 83.6 us
    pallas_call x1, Pallas kernels: 85.8 us -> 83.6 us  [local(): pl.pallas_call(functools.partial(kernel, n_sp, n_tp), out_shape=(jax.Shap...]
where the time goes in v8:
time: 85.8 us; the launch traced here: 85.7 us
  Pallas kernels  83.6 us (97%)
  other arithmetic  1.99 us (2%)
    pallas_call x1, Pallas kernels, local(): pl.pallas_call(functools.partial(kernel, n_sp, n_tp), out_shape=(jax.Shap...  83.6 us
    convert_element_type x1, other arithmetic, local(): return (latent.astype(f32) + gate * blended.astype(f32)).astype(bf16)  1.99 us

profile of v8, /device:TPU:33, one launch (start us, length us, event | category | flops | bytes accessed | tf_op | source)
XLA Modules:
  0.0 85.7 jit_solution(13673863298046906195)
XLA Ops:
  0.0 0.0 copy-start
  0.0 83.6 %shard_map.136 = (bf16[64,4096]{1,0:T(8,128)(2,1)}, f32[1,4096]{1,0:T(1,128)}) custom-call(bf16[64,4096]{1,0:T(8,128)(2,1)} %latent.1, bf16[24,4096]{1,0:T(8,128)(2,1)} %context.1, bf16[1,128]{1,0:T(2,128)(2,1)} %bitcast.10, f32[1,4096]{1,0:T(1,128)} %bitcast.8, bf16[128,512]{1,0:T(8,128)(2,1)} %shift_w.1, bf16[128,512]{1,0:T(8,128)(2,1)} %scale_w.1, ...), custom_call_target="tpu_custom_call" | custom-call | tf_op jit(solution)/shard_map/pallas_call | solution.py:717
  83.7 0.0 copy-done
  83.7 2.0 %add_convert_fusion = bf16[64,4096]{1,0:T(8,128)(2,1)} fusion(bf16[64,4096]{1,0:T(8,128)(2,1)} %get-tuple-element.8, bf16[64,4096]{1,0:T(8,128)(2,1)S(1)} %copy-done, f32[4096]{0:T(1024)} %bitcast.9), kind=kLoop, calls=%fused_computation | loop fusion | flops 1310720 | bytes 1589248 | tf_op jit(solution)/shard_map/convert_element_type | solution.py:797
Async XLA Ops:
  0.0 83.7 %copy-start = (bf16[64,4096]{1,0:T(8,128)(2,1)S(1)}, bf16[64,4096]{1,0:T(8,128)(2,1)}, u32[]{:S(2)}) copy-start(bf16[64,4096]{1,0:T(8,128)(2,1)} %latent.1) | copy-start | bytes 1572868

commit v9 on v8

--- a/solution.py
+++ b/solution.py
@@ -612,10 +612,8 @@
 
         attend(b)
         att_send(b)
-        if n >= 2:
-            att_take(order[n - 2])
-    att_take(order[-2])
-    att_take(order[-1])
+    for b in order:
+        att_take(b)
     for role, xx in ((0, x), (1, xl), (2, xr), (3, xo)):
         recv(att.at[xx * 2 + 1 - c], tsib_recv.at[role], {"tp": sib})
 

time: 85.8 us -> 84.1 us (0.980)
  Pallas kernels: 83.6 us -> 82 us
    pallas_call x1, Pallas kernels: 83.6 us -> 82 us  [local(): pl.pallas_call(functools.partial(kernel, n_sp, n_tp), out_shape=(jax.Shap...]
where the time goes in v9:
time: 84.1 us; the launch traced here: 84 us
  Pallas kernels  82 us (98%)
  other arithmetic  1.99 us (2%)
    pallas_call x1, Pallas kernels, local(): pl.pallas_call(functools.partial(kernel, n_sp, n_tp), out_shape=(jax.Shap...  82 us
    convert_element_type x1, other arithmetic, local(): return (latent.astype(f32) + gate * blended.astype(f32)).astype(bf16)  1.99 us

profile of v9, /device:TPU:33, one launch (start us, length us, event | category | flops | bytes accessed | tf_op | source)
XLA Modules:
  0.0 84.0 jit_solution(7064878347136047883)
XLA Ops:
  0.0 0.0 copy-start
  0.0 82.0 %shard_map.136 = (bf16[64,4096]{1,0:T(8,128)(2,1)}, f32[1,4096]{1,0:T(1,128)}) custom-call(bf16[64,4096]{1,0:T(8,128)(2,1)} %latent.1, bf16[24,4096]{1,0:T(8,128)(2,1)} %context.1, bf16[1,128]{1,0:T(2,128)(2,1)} %bitcast.10, f32[1,4096]{1,0:T(1,128)} %bitcast.8, bf16[128,512]{1,0:T(8,128)(2,1)} %shift_w.1, bf16[128,512]{1,0:T(8,128)(2,1)} %scale_w.1, ...), custom_call_target="tpu_custom_call" | custom-call | tf_op jit(solution)/shard_map/pallas_call | solution.py:715
  82.0 0.0 copy-done
  82.0 2.0 %add_convert_fusion = bf16[64,4096]{1,0:T(8,128)(2,1)} fusion(bf16[64,4096]{1,0:T(8,128)(2,1)} %get-tuple-element.8, bf16[64,4096]{1,0:T(8,128)(2,1)S(1)} %copy-done, f32[4096]{0:T(1024)} %bitcast.9), kind=kLoop, calls=%fused_computation | loop fusion | flops 1310720 | bytes 1589248 | tf_op jit(solution)/shard_map/convert_element_type | solution.py:795
Async XLA Ops:
  0.0 82.0 %copy-start = (bf16[64,4096]{1,0:T(8,128)(2,1)S(1)}, bf16[64,4096]{1,0:T(8,128)(2,1)}, u32[]{:S(2)}) copy-start(bf16[64,4096]{1,0:T(8,128)(2,1)} %latent.1) | copy-start | bytes 1572868
